TPU v7x, 32 devices: a whole 2x2x4 slice. The times are simulated.
32 devices in a mesh: sp: 8 (over z, x), tp: 4 (over y, core).
Axes of the slice: x: 2, y: 2, z: 4, core: 2. Of those that a mesh axis runs over, the one named last changes fastest.
Arguments:
- tokens: bfloat16 [4096, 2048], P(('sp', 'tp')), may hold values from -6 to 6
- input_norm_scale: bfloat16 [2048], replicated, may hold values from 0.099609375 to 1.8984375
- outer_gate_weight: bfloat16 [2048, 1024], P('sp', 'tp'), may hold values from -0.125 to 0.125
- inner_gate_weight: bfloat16 [2048, 1024], P('sp', 'tp'), may hold values from -0.125 to 0.125
- value_weight_matrix: bfloat16 [2048, 1024], P('sp', 'tp'), may hold values from -0.125 to 0.125
- output_gate_weight: bfloat16 [2048, 1024], P('sp', 'tp'), may hold values from -0.125 to 0.125
- state_input_weight: bfloat16 [2048, 1024], P('sp', 'tp'), may hold values from -0.125 to 0.125
- write_key_weight: bfloat16 [2048, 512], P('sp', 'tp'), may hold values from -0.125 to 0.125
- read_key_weight: bfloat16 [2048, 512], P('sp', 'tp'), may hold values from -0.125 to 0.125
- step_size_weight: bfloat16 [2048, 16], P(None, 'tp'), may hold values from -0.125 to 0.125
- gated_conv_weight: bfloat16 [3, 1024], P(None, 'tp'), may hold values from -3.5 to 3.5
- input_conv_weight: bfloat16 [4, 1024], P(None, 'tp'), may hold values from -3 to 3
- write_conv_weight: bfloat16 [4, 512], P(None, 'tp'), may hold values from -3 to 3
- read_conv_weight: bfloat16 [4, 512], P(None, 'tp'), may hold values from -3 to 3
- step_size_bias: float32 [16], P('tp'), may hold values from -1 to 0.5
- log_decay_rate: float32 [16], P('tp'), may hold values from -16 to -2.5, as said below
- decay_spikes: float32 [16, 4096], P('tp', 'sp'), may hold values from -1 to 0, as said below
- direct_path_weight: float32 [16], P('tp'), may hold values from 0.5 to 2
- head_norm_scale: bfloat16 [1024], P('tp'), may hold values from 0.099609375 to 1.8984375
- conv_output_weight: bfloat16 [1024, 2048], P('tp', 'sp'), may hold values from -0.125 to 0.125
- state_output_weight: bfloat16 [1024, 2048], P('tp', 'sp'), may hold values from -0.125 to 0.125
Outputs:
- mixed: bfloat16 [4096, 2048], P(('sp', 'tp'))
Inputs may be any that keep to these rules, and one draw needn't show every extreme that they name: `log_decay_rate`: one value a head. `decay_spikes`: never positive.
All inputs are finite; a program needn't handle non-finite values.
Results may differ from a plain program's by a relative error of at most 0.017.
Values may be sent and summed in bfloat16 or wider, within the bound.
A program may use at most 128 MiB of HBM per device.

v0:
```python
import functools

import jax
import jax.numpy as jnp
from jax import lax
from jax.experimental import pallas as pl
from jax.experimental.pallas import tpu as pltpu
from jax.sharding import PartitionSpec as P

HEAD_DIM = 64
STATE = 128
PLAIN_BLOCK = 64
CHUNK = 128
HALO = 16
QIN = 2
QOUT = 2
CORES = 2
epsilon = 1e-05
highest = lax.Precision.HIGHEST
f32 = jnp.float32
bf16 = jnp.bfloat16
MESH = pl.DeviceIdType.MESH


def nt(a, b, precision=None):
    return lax.dot_general(
        a, b, (((1,), (1,)), ((), ())), preferred_element_type=f32, precision=precision
    )


def silu(v):
    return v / (1.0 + jnp.exp(-v))


def kernel(
    n,
    T,
    tokens,
    in_scale,
    w_outer,
    w_inner,
    w_value,
    w_ogate,
    w_state,
    w_write,
    w_read,
    step_w,
    taps_conv,
    taps_in,
    taps_wr,
    taps_rd,
    bias,
    rate,
    spikes,
    direct,
    hscale,
    o_conv,
    o_state,
    out,
    wbuf,
    obuf,
    norm,
    acc,
    mixbuf,
    xbuf,
    wrbuf,
    rdbuf,
    ybuf,
    cumbuf,
    stbuf,
    st_send,
    st_recv,
    e_send,
    e_recv,
    pair_buf,
    apart,
    part,
    r1,
    p2,
    r2,
    loc_sem,
    ws_sem,
    wr_sem,
    os_sem,
    or_sem,
    ts_sem,
    tr_sem,
    h_sem,
    x_sem,
    e_sem,
    r1s_sem,
    r1r_sem,
    r2s_sem,
    r2r_sem,
):
    sp = lax.axis_index("sp")
    tp = lax.axis_index("tp")
    rows, width = tokens.shape
    kdim = w_outer.shape[0]
    cdim = w_outer.shape[1]
    half = wbuf.shape[3]
    length = rows * T
    heads_width = xbuf.shape[1]
    heads = heads_width // HEAD_DIM
    n_half = n // 2

    barrier = pltpu.get_barrier_semaphore()
    for d in range(1, n):
        pl.semaphore_signal(
            barrier, inc=1, device_id={"sp": lax.rem(sp + d, n)}, device_id_type=MESH
        )
    for d in range(1, T):
        pl.semaphore_signal(
            barrier, inc=1, device_id={"tp": lax.rem(tp + d, T)}, device_id_type=MESH
        )

    locals_ = []
    at = 0
    for ref in (w_outer, w_inner, w_value):
        locals_.append((ref, wbuf.at[0, 0, :, at : at + ref.shape[1]]))
        at += ref.shape[1]
    at = 0
    for ref in (w_ogate, w_state, w_write, w_read):
        locals_.append((ref, wbuf.at[0, 1, :, at : at + ref.shape[1]]))
        at += ref.shape[1]
    ohalf = obuf.shape[3]
    for way in range(2):
        cut = pl.ds(way * ohalf, ohalf)
        locals_.append((o_conv.at[:, cut], obuf.at[0, way, pl.ds(0, cdim)]))
        locals_.append((o_state.at[:, cut], obuf.at[0, way, pl.ds(cdim, heads_width)]))
    local_copies = [
        pltpu.make_async_copy(src, dst, loc_sem.at[i]) for i, (src, dst) in enumerate(locals_)
    ]
    for copy in local_copies:
        copy.start()

    def pos_of(index):
        odd = lax.rem(index, 2)
        low = lax.div(index, 2)
        return (1 - odd) * low + odd * (n - 1 - low)

    def index_of(pos):
        high = lax.div(pos, n_half)
        return (1 - high) * 2 * pos + high * (2 * (n - 1 - pos) + 1)

    pos = pos_of(sp)
    right = index_of(lax.rem(pos + 1, n))
    left = index_of(lax.rem(pos + n - 1, n))
    neighbour = (right, left)

    def owner_of(s, way):
        return index_of(lax.rem(pos + n - s, n) if way == 0 else lax.rem(pos + s, n))

    piece = kdim // QIN

    def w_copy(s, q, way):
        return pltpu.make_async_remote_copy(
            src_ref=wbuf.at[s, way, pl.ds(q * piece, piece)],
            dst_ref=wbuf.at[s + 1, way, pl.ds(q * piece, piece)],
            send_sem=ws_sem.at[s, q, way],
            recv_sem=wr_sem.at[s, q, way],
            device_id={"sp": neighbour[way]},
            device_id_type=MESH,
        )

    opiece = obuf.shape[2] // QOUT

    def o_copy(s, q, way):
        return pltpu.make_async_remote_copy(
            src_ref=obuf.at[s, way, pl.ds(q * opiece, opiece)],
            dst_ref=obuf.at[s + 1, way, pl.ds(q * opiece, opiece)],
            send_sem=os_sem.at[s, q, way],
            recv_sem=or_sem.at[s, q, way],
            device_id={"sp": neighbour[way]},
            device_id_type=MESH,
        )

    def forward(s):
        for q in range(QIN):
            for way in range(2):

                @pl.when(s > 0)
                def _():
                    w_copy(s - 1, q, way).wait_recv()

                @pl.when(s < n - 1)
                def _():
                    w_copy(s, q, way).start()

    def o_forward(s):
        for q in range(QOUT):
            for way in range(2):

                @pl.when(s > 0)
                def _():
                    o_copy(s - 1, q, way).wait_recv()

                @pl.when(s < n - 1)
                def _():
                    o_copy(s, q, way).start()

    own_at = pl.multiple_of(HALO + tp * rows, HALO)
    x = tokens[...].astype(f32)
    x = x * lax.rsqrt(jnp.mean(x * x, axis=1, keepdims=True) + epsilon)
    norm[pl.ds(own_at, rows), :] = (x * in_scale[...].astype(f32).reshape(1, width)).astype(bf16)
    acc[...] = jnp.zeros_like(acc)

    for copy in local_copies:
        copy.wait()
    pl.semaphore_wait(barrier, n - 1 + T - 1)

    forward(0)

    def t_copy(d):
        return pltpu.make_async_remote_copy(
            src_ref=norm.at[pl.ds(own_at, rows)],
            dst_ref=norm.at[pl.ds(own_at, rows)],
            send_sem=ts_sem.at[d],
            recv_sem=tr_sem.at[d],
            device_id={"tp": lax.rem(tp + d, T)},
            device_id_type=MESH,
        )

    for d in range(1, T):
        t_copy(d).start()

    mid = n_half - 1

    def ahead(s, carry):
        forward(s)
        return carry

    lax.fori_loop(1, max(mid, 1), ahead, 0)

    def t_wait(d):
        source = pl.multiple_of(HALO + lax.rem(tp + T - d, T) * rows, HALO)
        pltpu.make_async_remote_copy(
            src_ref=norm.at[pl.ds(source, rows)],
            dst_ref=norm.at[pl.ds(source, rows)],
            send_sem=ts_sem.at[d],
            recv_sem=tr_sem.at[d],
            device_id={"tp": lax.rem(tp + d, T)},
            device_id_type=MESH,
        ).wait_recv()

    for d in range(1, T):
        t_wait(d)

    def h_copy():
        return pltpu.make_async_remote_copy(
            src_ref=norm.at[pl.ds(length, HALO)],
            dst_ref=norm.at[pl.ds(0, HALO)],
            send_sem=h_sem.at[0],
            recv_sem=h_sem.at[1],
            device_id={"sp": lax.rem(sp + 1, n)},
            device_id_type=MESH,
        )

    @pl.when(sp < n - 1)
    def _():
        h_copy().start()

    forward(max(mid, 1))

    @pl.when(sp > 0)
    def _():
        h_copy().wait_recv()

    @pl.when(sp == 0)
    def _():
        norm[0:HALO, :] = jnp.zeros((HALO, width), bf16)

    def project(s):
        for way in range(2):
            at = pl.multiple_of(owner_of(s, way) * kdim, kdim)
            lhs = norm[:, pl.ds(at, kdim)]
            for c in range(0, half, 256):
                acc[:, way * half + c : way * half + c + 256] += jnp.dot(
                    lhs, wbuf[s, way, :, c : c + 256], preferred_element_type=f32
                )

    start = max(mid, 1)

    def body(s, carry):
        @pl.when(s > start)
        def _():
            forward(s)

        @pl.when(s == max(n - 2, start))
        def _():
            o_forward(0)

        project(s)

        @pl.when(s - start < start)
        def _():
            project(s - start)

        return carry

    lax.fori_loop(start, n, body, 0)

    def column(ref):
        index = lax.broadcasted_iota(jnp.int32, (heads, 1), 0)
        full = jnp.full((heads, 1), ref[0], f32)
        for h in range(1, heads):
            full = jnp.where(index == h, ref[h], full)
        return full

    step = jax.nn.softplus(jnp.dot(norm[HALO:, :], step_w[...], preferred_element_type=f32).T + column(bias))
    logs = -step * jnp.exp(column(rate)) + spikes[...]
    r_id = lax.broadcasted_iota(jnp.int32, (CHUNK, CHUNK), 0)
    c_id = lax.broadcasted_iota(jnp.int32, (CHUNK, CHUNK), 1)
    causal = r_id >= c_id
    lower = causal.astype(f32)
    eye = (r_id == c_id).astype(f32)
    lane = lax.broadcasted_iota(jnp.int32, (1, heads_width), 1)

    def spread(columns):
        full = jnp.broadcast_to(columns[:, 0:1], (columns.shape[0], heads_width))
        for h in range(1, heads):
            full = jnp.where(lane >= h * HEAD_DIM, columns[:, h : h + 1], full)
        return full

    def taps(u, weights):
        k_taps = weights.shape[0]
        w = weights[...].astype(f32)
        total = w[k_taps - 1 : k_taps] * u[8:]
        for k in range(k_taps - 1):
            total = total + w[k : k + 1] * pltpu.roll(u, k_taps - 1 - k, 0)[8:]
        return total

    blocks = length // CHUNK
    running = jnp.zeros((STATE, heads_width), f32)
    before = jnp.zeros((1, heads_width), f32)
    at_outer, at_inner, at_value, at_ogate, at_state = (i * cdim for i in range(5))
    at_write = 5 * cdim
    at_read = at_write + STATE
    for b in range(blocks):
        t0 = b * CHUNK
        take = slice(t0 + HALO - 8, t0 + HALO + CHUNK)
        own = slice(t0 + HALO, t0 + HALO + CHUNK)

        def field(begin, size, span):
            return acc[span, begin : begin + size].astype(bf16).astype(f32)

        product = field(at_inner, cdim, take) * field(at_value, cdim, take)
        mix = field(at_outer, cdim, own) * taps(product, taps_conv)
        apart[t0 : t0 + CHUNK, 0:cdim] = mix.astype(bf16)
        xs = silu(taps(field(at_state, cdim, take), taps_in))
        wr = silu(taps(field(at_write, STATE, take), taps_wr))
        rd = silu(taps(field(at_read, STATE, take), taps_rd))
        span = slice(t0, t0 + CHUNK)
        cum = nt(lower, logs[:, span], highest)
        steps = nt(eye, step[:, span], highest)
        cum_wide = spread(cum)
        weighted = xs * spread(steps)
        xbuf[span, :] = xs
        mixbuf[span, :] = weighted.astype(bf16)
        wrbuf[span, :] = wr.astype(bf16)
        rdbuf[span, :] = rd.astype(bf16)
        cumbuf[span, :] = cum_wide
        last = cum_wide[CHUNK - 1 : CHUNK]
        scaled = (weighted * jnp.exp(last - cum_wide)).astype(bf16)
        stbuf[b] = running
        running = running * jnp.exp(last) + jnp.dot(
            wr.T.astype(bf16), scaled, preferred_element_type=f32
        )
        before = before + last
    st_send[0:STATE, :] = running.astype(bf16)
    st_send[STATE:, :] = jnp.broadcast_to(jnp.exp(before), (HALO, heads_width)).astype(bf16)

    z = lax.div(sp, 2)
    second = lax.rem(sp, 2)
    depth = n_half

    def x_copy():
        return pltpu.make_async_remote_copy(
            src_ref=st_send,
            dst_ref=st_recv,
            send_sem=x_sem.at[0],
            recv_sem=x_sem.at[1],
            device_id={"sp": sp + 1 - 2 * second},
            device_id_type=MESH,
        )

    def e_copy():
        return pltpu.make_async_remote_copy(
            src_ref=e_send,
            dst_ref=e_recv,
            send_sem=e_sem.at[0],
            recv_sem=e_sem.at[1],
            device_id={"sp": lax.rem(sp + 2, n)},
            device_id_type=MESH,
        )

    x_copy().start()
    o_next = 1

    def within(b):
        t0 = b * CHUNK
        span = slice(t0, t0 + CHUNK)
        scores = nt(rdbuf[span, :], wrbuf[span, :])
        cum_t = lax.dot_general(
            logs[:, span], lower, (((1,), (1,)), ((), ())),
            preferred_element_type=f32, precision=highest,
        )
        for pair in range(0, heads_width, 128):
            both = []
            for h in range(pair // HEAD_DIM, (pair + 128) // HEAD_DIM):
                diff = cumbuf[span, h * HEAD_DIM : h * HEAD_DIM + 1] - cum_t[h : h + 1, :]
                damped = scores * jnp.exp(jnp.where(causal, diff, -1e30))
                both.append(
                    jnp.dot(
                        damped.astype(bf16), mixbuf[span, pair : pair + 128],
                        preferred_element_type=f32,
                    )
                )
            first = lax.broadcasted_iota(jnp.int32, (1, 128), 1) < HEAD_DIM
            ybuf[span, pair : pair + 128] = jnp.where(first, both[0], both[1])

    for b in range(blocks):
        if b % 2 == 0 and o_next < n:
            o_forward(o_next)
            o_next += 1
        within(b)
    x_copy().wait_recv()
    other = st_recv[0:STATE, :].astype(f32)
    other_decay = st_recv[STATE : STATE + 1, :].astype(f32)
    own_decay = jnp.exp(before)
    is_second = jnp.broadcast_to(second, (1, heads_width)) == 1
    pair_buf[0] = jnp.where(
        is_second, other * own_decay + running, running * other_decay + other
    )
    pair_buf[1] = jnp.where(is_second, other, jnp.zeros_like(other))
    pair_decay = own_decay * other_decay
    first_decay = jnp.where(is_second, other_decay, jnp.ones_like(other_decay))

    group = (
        lax.div(lax.broadcasted_iota(jnp.int32, (heads_width, heads_width), 0), HEAD_DIM)
        == lax.div(lax.broadcasted_iota(jnp.int32, (heads_width, heads_width), 1), HEAD_DIM)
    ).astype(bf16)
    direct_wide = jnp.full((1, heads_width), direct[0], f32)
    for h in range(1, heads):
        direct_wide = jnp.where(lane >= h * HEAD_DIM, direct[h], direct_wide)

    def finish():
        before = jnp.zeros((1, heads_width), f32)
        arriving = pair_buf[1] + first_decay * pair_buf[2]
        for b in range(blocks):
            t0 = b * CHUNK
            span = slice(t0, t0 + CHUNK)
            own = slice(t0 + HALO, t0 + HALO + CHUNK)
            cum_wide = cumbuf[span, :]
            entering = (stbuf[b] + jnp.exp(before) * arriving).astype(bf16)
            before = before + cum_wide[CHUNK - 1 : CHUNK]
            head_out = (
                ybuf[span, :]
                + jnp.dot(rdbuf[span, :], entering, preferred_element_type=f32) * jnp.exp(cum_wide)
                + direct_wide * xbuf[span, :]
            )
            og = acc[own, at_ogate : at_ogate + cdim].astype(bf16).astype(f32)
            gated = head_out * silu(og)
            square = jnp.dot((gated * gated).astype(bf16), group, preferred_element_type=f32)
            normalized = gated * lax.rsqrt(square * (1.0 / HEAD_DIM) + epsilon)
            apart[span, cdim:] = (normalized * hscale[...].astype(f32).reshape(1, heads_width)).astype(bf16)

    Y = T // CORES
    core = lax.rem(tp, CORES)
    chip = lax.div(tp, CORES)
    partner = chip * CORES + 1 - core
    ocols = 2 * ohalf

    def block_rows(y, c):
        return pl.ds(pl.multiple_of((y * CORES + c) * rows, rows), rows)

    def r1_copy(d, s):
        return pltpu.make_async_remote_copy(
            src_ref=part.at[s, block_rows(lax.rem(chip + d, Y), 1 - core)],
            dst_ref=r1.at[d, s],
            send_sem=r1s_sem.at[d, s],
            recv_sem=r1r_sem.at[d, s],
            device_id={"tp": partner},
            device_id_type=MESH,
        )

    def r2_copy(d, s):
        return pltpu.make_async_remote_copy(
            src_ref=p2.at[d, s],
            dst_ref=r2.at[d, s],
            send_sem=r2s_sem.at[d, s],
            recv_sem=r2r_sem.at[d, s],
            device_id={"tp": lax.rem(chip + d, Y) * CORES + core},
            device_id_type=MESH,
        )

    def reduce_far(s):
        for d in range(1, Y):
            r1_copy(d, s).wait_recv()
            mine = part[s, block_rows(lax.rem(chip + d, Y), core), :]
            p2[d, s] = (mine.astype(f32) + r1[d, s].astype(f32)).astype(bf16)
            r2_copy(d, s).start()

    def project_out(s, carry):
        for way in range(2):
            part[s, :, way * ohalf : (way + 1) * ohalf] = jnp.dot(
                apart[...], obuf[s, way], preferred_element_type=f32
            ).astype(bf16)
        for d in range(1, Y):
            r1_copy(d, s).start()
        r1_copy(0, s).start()

        @pl.when(s > 0)
        def _():
            reduce_far(s - 1)

        return carry

    def link(j, carry):
        @pl.when(z == j)
        def _():
            @pl.when(j == 0)
            def _():
                pair_buf[2] = jnp.zeros_like(pair_buf[2])

            @pl.when(j > 0)
            def _():
                e_copy().wait_recv()
                pair_buf[2] = e_recv[...].astype(f32)

            @pl.when(j < depth - 1)
            def _():
                e_send[...] = (pair_buf[2] * pair_decay + pair_buf[0]).astype(bf16)
                e_copy().start()

            finish()
            lax.fori_loop(0, o_next + j, project_out, 0)

        @pl.when(o_next + j < n)
        def _():
            o_forward(o_next + j)

            @pl.when(z <= j)
            def _():
                project_out(o_next + j, 0)

        return carry

    lax.fori_loop(0, depth, link, 0)

    def rest(s, carry):
        o_forward(s)
        project_out(s, 0)
        return carry

    lax.fori_loop(min(o_next + depth, n), n, rest, 0)
    reduce_far(n - 1)

    def collect(s, carry):
        r1_copy(0, s).wait_recv()
        total = part[s, block_rows(chip, core), :].astype(f32) + r1[0, s].astype(f32)
        for d in range(1, Y):
            r2_copy(d, s).wait_recv()
            total = total + r2[d, s].astype(f32)
        for way in range(2):
            at = pl.multiple_of(owner_of(s, way) * ocols + way * ohalf, ohalf)
            out[:, pl.ds(at, ohalf)] = total[:, way * ohalf : (way + 1) * ohalf].astype(bf16)
        return carry

    lax.fori_loop(0, n, collect, 0)

    def w_drain(s, carry):
        for way in range(2):
            for q in range(QIN):
                w_copy(s, q, way).wait_send()
            for q in range(QOUT):
                o_copy(s, q, way).wait_send()
        return carry

    lax.fori_loop(0, n - 1, w_drain, 0)
    for d in range(1, T):
        t_copy(d).wait_send()

    @pl.when(sp < n - 1)
    def _():
        h_copy().wait_send()

    x_copy().wait_send()

    @pl.when(z < depth - 1)
    def _():
        e_copy().wait_send()

    def r_drain(s, carry):
        for d in range(Y):
            r1_copy(d, s).wait_send()
        for d in range(1, Y):
            r2_copy(d, s).wait_send()
        return carry

    lax.fori_loop(0, n, r_drain, 0)


def shifted(shard, axis, by):
    devices = lax.axis_size(axis)
    pairs = [(i, i + by) for i in range(devices) if 0 <= i + by < devices]
    return lax.ppermute(shard, axis, pairs)


def prefix(shard, axis, combine, identity):
    devices, index = (lax.axis_size(axis), lax.axis_index(axis))
    everything = jax.tree.map(
        lambda part, kind: lax.all_gather(part.astype(kind), axis),
        shard,
        (jnp.bfloat16, jnp.bfloat16),
    )
    start = jax.tree.map(
        lambda part, zero: jnp.broadcast_to(jnp.asarray(zero, part.dtype), part.shape),
        shard,
        identity,
    )

    def turn(k, before):
        reached = k < index
        new = combine(
            before, jax.tree.map(lambda part, own: part[k].astype(own.dtype), everything, shard)
        )
        return jax.tree.map(lambda a, b: jnp.where(reached, a, b), new, before)

    return lax.fori_loop(0, devices, turn, start)


def causal_taps(values, rim_rows, tap_weights):
    tap_count = tap_weights.shape[0]
    length = values.shape[0]
    padded = jnp.concatenate([rim_rows, values], axis=0)
    running = tap_weights[0] * padded[0:length]
    for offset in range(1, tap_count):
        running = running + tap_weights[offset] * padded[offset : offset + length]
    return running


def combine_states(earlier, later):
    return (earlier[0] * later[0], earlier[1] * later[0][:, None, None] + later[1])


def plain_path(
    tokens,
    input_norm_scale,
    outer_gate_weight,
    inner_gate_weight,
    value_weight_matrix,
    output_gate_weight,
    state_input_weight,
    write_key_weight,
    read_key_weight,
    step_size_weight,
    gated_conv_weight,
    input_conv_weight,
    write_conv_weight,
    read_conv_weight,
    step_size_bias,
    log_decay_rate,
    decay_spikes,
    direct_path_weight,
    head_norm_scale,
    conv_output_weight,
    state_output_weight,
):
    token_rows = tokens.astype(jnp.float32)
    scaled = token_rows * lax.rsqrt(
        jnp.mean(token_rows * token_rows, axis=1, keepdims=True) + epsilon
    )
    normed_own = (scaled * input_norm_scale.astype(jnp.float32)).astype(jnp.bfloat16)
    normed = lax.all_gather(normed_own, "tp", axis=0, tiled=True)
    length = normed.shape[0]
    pieces = (
        lax.all_gather(outer_gate_weight, "sp", axis=0, tiled=True),
        lax.all_gather(inner_gate_weight, "sp", axis=0, tiled=True),
        lax.all_gather(value_weight_matrix, "sp", axis=0, tiled=True),
        lax.all_gather(output_gate_weight, "sp", axis=0, tiled=True),
        lax.all_gather(state_input_weight, "sp", axis=0, tiled=True),
        lax.all_gather(write_key_weight, "sp", axis=0, tiled=True),
        lax.all_gather(read_key_weight, "sp", axis=0, tiled=True),
    )
    projected = tuple(
        (jnp.dot(normed, weight_rows, preferred_element_type=jnp.float32) for weight_rows in pieces)
    )
    outer_gate, inner_gate, conv_input, out_gate, state_input, write_keys, read_keys = [
        member.astype(jnp.bfloat16) for member in projected
    ]
    step_raw = jnp.dot(normed, step_size_weight, preferred_element_type=jnp.float32)
    short_rim = gated_conv_weight.shape[0] - 1
    state_rim = input_conv_weight.shape[0] - 1
    rim_rows = shifted(
        (
            inner_gate[length - short_rim :],
            conv_input[length - short_rim :],
            state_input[length - state_rim :],
            write_keys[length - state_rim :],
            read_keys[length - state_rim :],
        ),
        "sp",
        1,
    )
    product = inner_gate.astype(jnp.float32) * conv_input.astype(jnp.float32)
    rim_product = rim_rows[0].astype(jnp.float32) * rim_rows[1].astype(jnp.float32)
    mixer_part = (
        outer_gate.astype(jnp.float32)
        * causal_taps(product, rim_product, gated_conv_weight.astype(jnp.float32))
    ).astype(jnp.bfloat16)
    seq_input = jax.nn.silu(
        causal_taps(
            state_input.astype(jnp.float32),
            rim_rows[2].astype(jnp.float32),
            input_conv_weight.astype(jnp.float32),
        )
    )
    seq_write = jax.nn.silu(
        causal_taps(
            write_keys.astype(jnp.float32),
            rim_rows[3].astype(jnp.float32),
            write_conv_weight.astype(jnp.float32),
        )
    )
    seq_read = jax.nn.silu(
        causal_taps(
            read_keys.astype(jnp.float32),
            rim_rows[4].astype(jnp.float32),
            read_conv_weight.astype(jnp.float32),
        )
    )
    discrete_step = jax.nn.softplus(step_raw + step_size_bias[None, :])
    step_logarithm = discrete_step * (-jnp.exp(log_decay_rate))[None, :] + decay_spikes.T
    heads_here = discrete_step.shape[1]
    groups_here = seq_write.shape[1] // STATE
    per_group = heads_here // groups_here
    blocks = length // PLAIN_BLOCK
    input_blocks = seq_input.reshape(blocks, PLAIN_BLOCK, heads_here, HEAD_DIM)
    weighted = input_blocks * discrete_step.reshape(blocks, PLAIN_BLOCK, heads_here, 1)
    write_blocks = jnp.repeat(
        seq_write.reshape(blocks, PLAIN_BLOCK, groups_here, STATE), per_group, axis=2
    )
    read_blocks = jnp.repeat(seq_read.reshape(blocks, PLAIN_BLOCK, groups_here, STATE), per_group, axis=2)
    cumulative = jnp.cumsum(step_logarithm.reshape(blocks, PLAIN_BLOCK, heads_here), axis=1)
    causal = lax.broadcasted_iota(jnp.int32, (PLAIN_BLOCK, PLAIN_BLOCK), 0) >= lax.broadcasted_iota(
        jnp.int32, (PLAIN_BLOCK, PLAIN_BLOCK), 1
    )
    scores = jnp.einsum("clhm,cshm->clsh", read_blocks, write_blocks, precision=highest)
    damping = jnp.exp(
        jnp.where(
            causal[None, :, :, None],
            cumulative[:, :, None, :] - cumulative[:, None, :, :],
            -jnp.inf,
        )
    )
    within_block = jnp.einsum("clsh,cshp->clhp", scores * damping, weighted, precision=highest)
    to_end = jnp.exp(cumulative[:, -1:, :] - cumulative)
    block_states = jnp.einsum(
        "cshm,cshp->chpm", write_blocks * to_end[..., None], weighted, precision=highest
    )
    block_logs = cumulative[:, -1, :]

    def advance(carried_state, inputs):
        contribution, block_log = inputs
        return (carried_state * jnp.exp(block_log)[:, None, None] + contribution, carried_state)

    own_total, own_before = lax.scan(
        advance, jnp.zeros(block_states.shape[1:], jnp.float32), (block_states, block_logs)
    )
    total_log = jnp.sum(block_logs, axis=0)
    arriving = prefix(
        (jnp.exp(total_log), own_total),
        "sp",
        combine_states,
        (jnp.ones_like(total_log), jnp.zeros_like(own_total)),
    )[1]
    before_logs = jnp.cumsum(block_logs, axis=0) - block_logs
    entering = own_before + jnp.exp(before_logs)[:, :, None, None] * arriving[None]
    from_before = (
        jnp.einsum("clhm,chpm->clhp", read_blocks, entering, precision=highest)
        * jnp.exp(cumulative)[..., None]
    )
    head_out = within_block + from_before + direct_path_weight[None, None, :, None] * input_blocks
    head_out = head_out.reshape(length, heads_here * HEAD_DIM)
    gated_heads = (head_out * jax.nn.silu(out_gate.astype(jnp.float32))).reshape(
        length, heads_here, HEAD_DIM
    )
    normalized = gated_heads * lax.rsqrt(
        jnp.mean(gated_heads * gated_heads, axis=2, keepdims=True) + epsilon
    )
    state_part = (
        normalized.reshape(length, heads_here * HEAD_DIM) * head_norm_scale.astype(jnp.float32)
    ).astype(jnp.bfloat16)
    wide_mixer, wide_state = (
        lax.all_gather(conv_output_weight, "sp", axis=1, tiled=True),
        lax.all_gather(state_output_weight, "sp", axis=1, tiled=True),
    )
    return lax.psum_scatter(
        (
            jnp.dot(mixer_part, wide_mixer, preferred_element_type=jnp.float32)
            + jnp.dot(state_part, wide_state, preferred_element_type=jnp.float32)
        ).astype(jnp.bfloat16),
        "tp",
        scatter_dimension=0,
        tiled=True,
    )


def per_device(
    tokens, input_norm_scale, outer_gate_weight, inner_gate_weight, value_weight_matrix,
    output_gate_weight, state_input_weight, write_key_weight, read_key_weight, step_size_weight,
    gated_conv_weight, input_conv_weight, write_conv_weight, read_conv_weight, step_size_bias,
    log_decay_rate, decay_spikes, direct_path_weight, head_norm_scale, conv_output_weight,
    state_output_weight,
):
    n, T = lax.axis_size("sp"), lax.axis_size("tp")
    rows, width = tokens.shape
    kdim, cdim = outer_gate_weight.shape
    heads = step_size_bias.shape[0]
    hw = heads * HEAD_DIM
    half = 3 * cdim
    length = rows * T
    ocols = conv_output_weight.shape[1]
    if kdim % 128 or ocols % 256 or n % 2 or T % CORES or write_key_weight.shape[1] != STATE:
        return plain_path(
            tokens, input_norm_scale, outer_gate_weight, inner_gate_weight,
            value_weight_matrix, output_gate_weight, state_input_weight, write_key_weight,
            read_key_weight, step_size_weight, gated_conv_weight, input_conv_weight,
            write_conv_weight, read_conv_weight, step_size_bias, log_decay_rate, decay_spikes,
            direct_path_weight, head_norm_scale, conv_output_weight, state_output_weight,
        )
    Y = T // CORES
    vm = pl.BlockSpec(memory_space=pltpu.VMEM)
    sm = pl.BlockSpec(memory_space=pltpu.SMEM)
    hbm = pl.BlockSpec(memory_space=pl.ANY)
    dma = pltpu.SemaphoreType.DMA
    return pl.pallas_call(
        functools.partial(kernel, n, T),
        out_shape=jax.ShapeDtypeStruct((rows, width), bf16),
        in_specs=[vm] * 2 + [hbm] * 7 + [vm] * 5 + [sm] * 2 + [vm, sm, vm] + [hbm] * 2,
        out_specs=vm,
        scratch_shapes=[
            pltpu.VMEM((n, 2, kdim, half), bf16),
            pltpu.VMEM((n, 2, cdim + hw, ocols // 2), bf16),
            pltpu.VMEM((HALO + length, width), bf16),
            pltpu.VMEM((HALO + length, 2 * half), f32),
            pltpu.VMEM((length, hw), bf16),
            pltpu.VMEM((length, hw), f32),
            pltpu.VMEM((length, STATE), bf16),
            pltpu.VMEM((length, STATE), bf16),
            pltpu.VMEM((length, hw), f32),
            pltpu.VMEM((length, hw), f32),
            pltpu.VMEM((length // CHUNK, STATE, hw), f32),
            pltpu.VMEM((STATE + HALO, hw), bf16),
            pltpu.VMEM((STATE + HALO, hw), bf16),
            pltpu.VMEM((STATE, hw), bf16),
            pltpu.VMEM((STATE, hw), bf16),
            pltpu.VMEM((3, STATE, hw), f32),
            pltpu.VMEM((length, cdim + hw), bf16),
            pltpu.VMEM((n, length, ocols), bf16),
            pltpu.VMEM((Y, n, rows, ocols), bf16),
            pltpu.VMEM((Y, n, rows, ocols), bf16),
            pltpu.VMEM((Y, n, rows, ocols), bf16),
            dma((11,)),
            dma((n, QIN, 2)),
            dma((n, QIN, 2)),
            dma((n, QOUT, 2)),
            dma((n, QOUT, 2)),
            dma((T,)),
            dma((T,)),
            dma((2,)),
            dma((2,)),
            dma((2,)),
            dma((Y, n)),
            dma((Y, n)),
            dma((Y, n)),
            dma((Y, n)),
        ],
        compiler_params=pltpu.CompilerParams(
            collective_id=0, has_side_effects=True, vmem_limit_bytes=62 * 1024 * 1024
        ),
    )(
        tokens, input_norm_scale, outer_gate_weight, inner_gate_weight,
        value_weight_matrix, output_gate_weight, state_input_weight, write_key_weight,
        read_key_weight, step_size_weight, gated_conv_weight, input_conv_weight, write_conv_weight,
        read_conv_weight, step_size_bias, log_decay_rate, decay_spikes, direct_path_weight,
        head_norm_scale,
        conv_output_weight, state_output_weight,
    )


def solution(mesh):
    placed = (
        (P(("sp", "tp"), None), P())
        + (P("sp", "tp"),) * 7
        + (P(None, "tp"),) * 5
        + (P("tp"), P("tp"), P("tp", "sp"), P("tp"), P("tp"), P("tp", "sp"), P("tp", "sp"))
    )
    return jax.shard_map(
        per_device, mesh=mesh, in_specs=placed, out_specs=P(("sp", "tp"), None), check_vma=False
    )
```

profile of v0, /device:TPU:0, one launch (start us, length us, event | category | flops | bytes accessed | tf_op | source)
XLA Modules:
  0.0 112.6 jit_solution(14108800712061375082)
XLA Ops:
  0.0 1.8 %copy.22.step_w = bf16[2048,4]{1,0:T(8,128)(2,1)} copy(bf16[2048,4]{0,1:T(4,128)(2,1)} %param.30) | data formatting | bytes 32768 | tf_op args[9]
  1.8 109.0 %shard_map.199 = bf16[128,2048]{1,0:T(8,128)(2,1)} custom-call(bf16[128,2048]{1,0:T(8,128)(2,1)} %tokens.1, bf16[2048]{0:T(1024)(128)(2,1)} %in_scale.1, bf16[256,256]{1,0:T(8,128)(2,1)} %w_outer.1, bf16[256,256]{1,0:T(8,128)(2,1)} %w_inner.1, bf16[256,256]{1,0:T(8,128)(2,1)} %w_value.1, bf16[256,256]{1,0:T(8,128)(2,1)} %w_ogate.1, ...), custom_call_target="tpu_custom_call" | custom-call | tf_op jit(solution)/shard_map/pallas_call | solution.py:838
  110.7 1.9 %copy.24 = bf16[128,2048]{1,0:T(8,128)(2,1)} copy(bf16[128,2048]{1,0:T(8,128)(2,1)} %shard_map.199) | data formatting | bytes 1048576
where the time goes:
time: 113 us
  Pallas kernels  109 us (96%)
  local copies, waits for them, and re-layouts  3.65 us (3%)
    pallas_call x1, Pallas kernels, per_device(): pl.pallas_call(functools.partial(kernel, n, T), out_shape=jax.ShapeDtypeS...  109 us
    unnamed x2, local copies, waits for them, and re-layouts  3.65 us

commit v1 on v0

--- a/solution.py
+++ b/solution.py
@@ -12,8 +12,10 @@
 PLAIN_BLOCK = 64
 CHUNK = 128
 HALO = 16
-QIN = 2
-QOUT = 2
+PIECES_S = 4
+PIECES_R = 8
+PIECES_O = 4
+PIECES_T = 2
 CORES = 2
 epsilon = 1e-05
 highest = lax.Precision.HIGHEST
@@ -32,77 +34,86 @@
     return v / (1.0 + jnp.exp(-v))
 
 
+class Ring:
+    def __init__(self, n, pieces, buf, send, recv, neighbour):
+        self.n, self.pieces, self.buf = n, pieces, buf
+        self.send_sem, self.recv_sem, self.neighbour = send, recv, neighbour
+        self.rows = buf.shape[1] // pieces
+        self.waited = set()
+
+    def copy(self, s, q, way):
+        n = self.n
+        src, dst = (s, s + 1) if way == 0 else ((n - s) % n, n - 1 - s)
+        cut = pl.ds(q * self.rows, self.rows)
+        return pltpu.make_async_remote_copy(
+            src_ref=self.buf.at[src, cut],
+            dst_ref=self.buf.at[dst, cut],
+            send_sem=self.send_sem.at[s, q, way],
+            recv_sem=self.recv_sem.at[s, q, way],
+            device_id={"sp": self.neighbour[way]},
+            device_id_type=MESH,
+        )
+
+    def ways(self, s, q):
+        if s < self.n // 2 - 1:
+            return (0, 1)
+        return (0,) if q < self.pieces // 2 else (1,)
+
+    def arrive(self, s, q, way):
+        if (s, q, way) not in self.waited:
+            self.waited.add((s, q, way))
+            self.copy(s, q, way).wait_recv()
+
+    def forward(self, s, q):
+        for way in self.ways(s, q):
+            if s > 0:
+                self.arrive(s - 1, q, way)
+            self.copy(s, q, way).start()
+
+    def need(self, slot):
+        last = self.n // 2
+        for q in range(self.pieces):
+            if 0 < slot < last:
+                self.arrive(slot - 1, q, 0)
+            elif slot > last:
+                self.arrive(self.n - slot - 1, q, 1)
+            elif slot == last:
+                self.arrive(last - 1, q, self.ways(last - 1, q)[0])
+
+    def order(self, first):
+        return [(s, q) for s in range(first, self.n // 2) for q in range(self.pieces)]
+
+    def drain(self):
+        for s, q in self.order(0):
+            for way in self.ways(s, q):
+                self.copy(s, q, way).wait_send()
+
+
 def kernel(
     n,
     T,
-    tokens,
-    in_scale,
-    w_outer,
-    w_inner,
-    w_value,
-    w_ogate,
-    w_state,
-    w_write,
-    w_read,
-    step_w,
-    taps_conv,
-    taps_in,
-    taps_wr,
-    taps_rd,
-    bias,
-    rate,
-    spikes,
-    direct,
-    hscale,
-    o_conv,
-    o_state,
-    out,
-    wbuf,
-    obuf,
-    norm,
-    acc,
-    mixbuf,
-    xbuf,
-    wrbuf,
-    rdbuf,
-    ybuf,
-    cumbuf,
-    stbuf,
-    st_send,
-    st_recv,
-    e_send,
-    e_recv,
-    pair_buf,
-    apart,
-    part,
-    r1,
-    p2,
-    r2,
-    loc_sem,
-    ws_sem,
-    wr_sem,
-    os_sem,
-    or_sem,
-    ts_sem,
-    tr_sem,
-    h_sem,
-    x_sem,
-    e_sem,
-    r1s_sem,
-    r1r_sem,
-    r2s_sem,
-    r2r_sem,
+    tokens_h, in_scale_h, w_outer, w_inner, w_value, w_ogate, w_state, w_write, w_read,
+    step_w_h, taps_conv_h, taps_in_h, taps_wr_h, taps_rd_h,
+    bias, rate, spikes_h, direct, hscale_h, o_conv, o_state,
+    near, far,
+    tokens, in_scale, step_w, taps_conv, taps_in, taps_wr, taps_rd, spikes, hscale,
+    sbuf, rbuf, obuf, norm, acc_s, acc_r, mixbuf, xbuf, wrbuf, rdbuf, ybuf, cumbuf, stbuf,
+    st_send, st_recv, e_send, e_recv, pair_buf, apart, part, r1, p2, nbuf,
+    loc_sem, ss_sem, sr_sem, rs_sem, rr_sem, os_sem, or_sem,
+    ts_sem, tr_sem, us_sem, ur_sem, h_sem, g_sem, x_sem, e_sem,
+    r1s_sem, r1r_sem, r2s_sem, r2r_sem, near_sem,
 ):
     sp = lax.axis_index("sp")
     tp = lax.axis_index("tp")
     rows, width = tokens.shape
     kdim = w_outer.shape[0]
     cdim = w_outer.shape[1]
-    half = wbuf.shape[3]
     length = rows * T
     heads_width = xbuf.shape[1]
     heads = heads_width // HEAD_DIM
+    ocols = obuf.shape[2]
     n_half = n // 2
+    Y = T // CORES
 
     barrier = pltpu.get_barrier_semaphore()
     for d in range(1, n):
@@ -114,25 +125,38 @@
             barrier, inc=1, device_id={"tp": lax.rem(tp + d, T)}, device_id_type=MESH
         )
 
-    locals_ = []
-    at = 0
-    for ref in (w_outer, w_inner, w_value):
-        locals_.append((ref, wbuf.at[0, 0, :, at : at + ref.shape[1]]))
-        at += ref.shape[1]
-    at = 0
-    for ref in (w_ogate, w_state, w_write, w_read):
-        locals_.append((ref, wbuf.at[0, 1, :, at : at + ref.shape[1]]))
-        at += ref.shape[1]
-    ohalf = obuf.shape[3]
-    for way in range(2):
-        cut = pl.ds(way * ohalf, ohalf)
-        locals_.append((o_conv.at[:, cut], obuf.at[0, way, pl.ds(0, cdim)]))
-        locals_.append((o_state.at[:, cut], obuf.at[0, way, pl.ds(cdim, heads_width)]))
-    local_copies = [
-        pltpu.make_async_copy(src, dst, loc_sem.at[i]) for i, (src, dst) in enumerate(locals_)
-    ]
-    for copy in local_copies:
-        copy.start()
+    def pack(refs, dst, rows_too=False):
+        pairs, at = [], 0
+        for ref in refs:
+            if rows_too:
+                pairs.append((ref, dst.at[0, pl.ds(at, ref.shape[0])]))
+                at += ref.shape[0]
+            else:
+                pairs.append((ref, dst.at[0, :, pl.ds(at, ref.shape[1])]))
+                at += ref.shape[1]
+        return pairs
+
+    groups = {
+        "s": pack((w_state, w_write, w_read), sbuf),
+        "t": [(tokens_h, tokens), (in_scale_h, in_scale)],
+        "r": pack((w_ogate, w_outer, w_inner, w_value), rbuf),
+        "v": [
+            (step_w_h, step_w), (taps_conv_h, taps_conv), (taps_in_h, taps_in),
+            (taps_wr_h, taps_wr), (taps_rd_h, taps_rd), (spikes_h, spikes), (hscale_h, hscale),
+        ],
+        "o": pack((o_conv, o_state), obuf, True),
+    }
+    local, index = {}, 0
+    for name, pairs in groups.items():
+        local[name] = []
+        for src, dst in pairs:
+            local[name].append(pltpu.make_async_copy(src, dst, loc_sem.at[index]))
+            local[name][-1].start()
+            index += 1
+
+    def landed(name):
+        for copy in local[name]:
+            copy.wait()
 
     def pos_of(index):
         odd = lax.rem(index, 2)
@@ -144,107 +168,45 @@
         return (1 - high) * 2 * pos + high * (2 * (n - 1 - pos) + 1)
 
     pos = pos_of(sp)
-    right = index_of(lax.rem(pos + 1, n))
-    left = index_of(lax.rem(pos + n - 1, n))
-    neighbour = (right, left)
-
-    def owner_of(s, way):
-        return index_of(lax.rem(pos + n - s, n) if way == 0 else lax.rem(pos + s, n))
-
-    piece = kdim // QIN
-
-    def w_copy(s, q, way):
+    neighbour = (index_of(lax.rem(pos + 1, n)), index_of(lax.rem(pos + n - 1, n)))
+
+    def owner_of(slot):
+        return index_of(lax.rem(pos + n - slot, n))
+
+    ring_s = Ring(n, PIECES_S, sbuf, ss_sem, sr_sem, neighbour)
+    ring_r = Ring(n, PIECES_R, rbuf, rs_sem, rr_sem, neighbour)
+    ring_o = Ring(n, PIECES_O, obuf, os_sem, or_sem, neighbour)
+
+    own_at = pl.multiple_of(HALO + tp * rows, HALO)
+    core = lax.rem(tp, CORES)
+    chip = lax.div(tp, CORES)
+    partner = chip * CORES + 1 - core
+    prow = rows // PIECES_T
+
+    def at_rows(block, q):
+        return norm.at[pl.ds(pl.multiple_of(HALO + block * rows + q * prow, HALO), prow)]
+
+    def t_copy(d, q):
+        device = partner if d == 0 else lax.rem(chip + d, Y) * CORES + core
         return pltpu.make_async_remote_copy(
-            src_ref=wbuf.at[s, way, pl.ds(q * piece, piece)],
-            dst_ref=wbuf.at[s + 1, way, pl.ds(q * piece, piece)],
-            send_sem=ws_sem.at[s, q, way],
-            recv_sem=wr_sem.at[s, q, way],
-            device_id={"sp": neighbour[way]},
+            src_ref=at_rows(tp, q),
+            dst_ref=at_rows(tp, q),
+            send_sem=ts_sem.at[d, q],
+            recv_sem=tr_sem.at[d, q],
+            device_id={"tp": device},
             device_id_type=MESH,
         )
 
-    opiece = obuf.shape[2] // QOUT
-
-    def o_copy(s, q, way):
+    def u_copy(d, q):
+        block = lax.rem(chip + Y - d, Y) * CORES + core
         return pltpu.make_async_remote_copy(
-            src_ref=obuf.at[s, way, pl.ds(q * opiece, opiece)],
-            dst_ref=obuf.at[s + 1, way, pl.ds(q * opiece, opiece)],
-            send_sem=os_sem.at[s, q, way],
-            recv_sem=or_sem.at[s, q, way],
-            device_id={"sp": neighbour[way]},
+            src_ref=at_rows(block, q),
+            dst_ref=at_rows(block, q),
+            send_sem=us_sem.at[d, q],
+            recv_sem=ur_sem.at[d, q],
+            device_id={"tp": partner},
             device_id_type=MESH,
         )
-
-    def forward(s):
-        for q in range(QIN):
-            for way in range(2):
-
-                @pl.when(s > 0)
-                def _():
-                    w_copy(s - 1, q, way).wait_recv()
-
-                @pl.when(s < n - 1)
-                def _():
-                    w_copy(s, q, way).start()
-
-    def o_forward(s):
-        for q in range(QOUT):
-            for way in range(2):
-
-                @pl.when(s > 0)
-                def _():
-                    o_copy(s - 1, q, way).wait_recv()
-
-                @pl.when(s < n - 1)
-                def _():
-                    o_copy(s, q, way).start()
-
-    own_at = pl.multiple_of(HALO + tp * rows, HALO)
-    x = tokens[...].astype(f32)
-    x = x * lax.rsqrt(jnp.mean(x * x, axis=1, keepdims=True) + epsilon)
-    norm[pl.ds(own_at, rows), :] = (x * in_scale[...].astype(f32).reshape(1, width)).astype(bf16)
-    acc[...] = jnp.zeros_like(acc)
-
-    for copy in local_copies:
-        copy.wait()
-    pl.semaphore_wait(barrier, n - 1 + T - 1)
-
-    forward(0)
-
-    def t_copy(d):
-        return pltpu.make_async_remote_copy(
-            src_ref=norm.at[pl.ds(own_at, rows)],
-            dst_ref=norm.at[pl.ds(own_at, rows)],
-            send_sem=ts_sem.at[d],
-            recv_sem=tr_sem.at[d],
-            device_id={"tp": lax.rem(tp + d, T)},
-            device_id_type=MESH,
-        )
-
-    for d in range(1, T):
-        t_copy(d).start()
-
-    mid = n_half - 1
-
-    def ahead(s, carry):
-        forward(s)
-        return carry
-
-    lax.fori_loop(1, max(mid, 1), ahead, 0)
-
-    def t_wait(d):
-        source = pl.multiple_of(HALO + lax.rem(tp + T - d, T) * rows, HALO)
-        pltpu.make_async_remote_copy(
-            src_ref=norm.at[pl.ds(source, rows)],
-            dst_ref=norm.at[pl.ds(source, rows)],
-            send_sem=ts_sem.at[d],
-            recv_sem=tr_sem.at[d],
-            device_id={"tp": lax.rem(tp + d, T)},
-            device_id_type=MESH,
-        ).wait_recv()
-
-    for d in range(1, T):
-        t_wait(d)
 
     def h_copy():
         return pltpu.make_async_remote_copy(
@@ -256,49 +218,125 @@
             device_id_type=MESH,
         )
 
-    @pl.when(sp < n - 1)
+    def g_copy(d):
+        return pltpu.make_async_remote_copy(
+            src_ref=norm.at[pl.ds(0, HALO)],
+            dst_ref=norm.at[pl.ds(0, HALO)],
+            send_sem=g_sem.at[0, d],
+            recv_sem=g_sem.at[1, d],
+            device_id={"tp": d},
+            device_id_type=MESH,
+        )
+
+    last_tp = tp == T - 1
+
+    landed("s")
+    pl.semaphore_wait(barrier, n - 1 + T - 1)
+    for q in range(PIECES_S):
+        ring_s.forward(0, q)
+    landed("t")
+    x = tokens[...].astype(f32)
+    x = x * lax.rsqrt(jnp.mean(x * x, axis=1, keepdims=True) + epsilon)
+    norm[pl.ds(own_at, rows), :] = (x * in_scale[...].astype(f32).reshape(1, width)).astype(bf16)
+    for q in range(PIECES_T):
+        for d in range(1, Y):
+            t_copy(d, q).start()
+        t_copy(0, q).start()
+
+    @pl.when(last_tp & (sp < n - 1))
     def _():
         h_copy().start()
 
-    forward(max(mid, 1))
-
-    @pl.when(sp > 0)
-    def _():
-        h_copy().wait_recv()
+    landed("r")
+    r_own = [(0, q) for q in range(PIECES_R)]
+    ring_r.forward(*r_own.pop(0))
+
+    def t_forward(q):
+        for d in range(1, Y):
+            t_copy(d, q).wait_recv()
+            u_copy(d, q).start()
+
+    s_list = ring_s.order(1)
+    hops = [s_list[i : i + PIECES_S] for i in range(0, len(s_list), PIECES_S)]
+    for i, hop in enumerate(hops):
+        for j, item in enumerate(hop):
+            ring_s.forward(*item)
+            if i == 1 and j == 0:
+                t_forward(0)
+            if i == 1 and j == 2:
+                for q in range(1, PIECES_T):
+                    t_forward(q)
+        if i == 0:
+
+            @pl.when(last_tp & (sp > 0))
+            def _():
+                h_copy().wait_recv()
+                for d in range(T - 1):
+                    g_copy(d).start()
+
+        if i < len(hops) - 1:
+            ring_r.forward(*r_own.pop(0))
+    while r_own:
+        ring_r.forward(*r_own.pop(0))
+
+    r_list = ring_r.order(1)
+    o_list = []
+
+    def pump(count):
+        for _ in range(count):
+            if r_list:
+                ring_r.forward(*r_list.pop(0))
+            elif o_list:
+                ring_o.forward(*o_list.pop(0))
+
+    for q in range(PIECES_T):
+        t_copy(0, q).wait_recv()
+        for d in range(1, Y):
+            pltpu.make_async_remote_copy(
+                src_ref=at_rows(lax.rem(chip + Y - d, Y) * CORES + 1 - core, q),
+                dst_ref=at_rows(lax.rem(chip + Y - d, Y) * CORES + 1 - core, q),
+                send_sem=us_sem.at[d, q],
+                recv_sem=ur_sem.at[d, q],
+                device_id={"tp": partner},
+                device_id_type=MESH,
+            ).wait_recv()
+    for d in range(T - 1):
+
+        @pl.when((tp == d) & (sp > 0))
+        def _():
+            g_copy(d).wait_recv()
 
     @pl.when(sp == 0)
     def _():
         norm[0:HALO, :] = jnp.zeros((HALO, width), bf16)
 
-    def project(s):
-        for way in range(2):
-            at = pl.multiple_of(owner_of(s, way) * kdim, kdim)
-            lhs = norm[:, pl.ds(at, kdim)]
-            for c in range(0, half, 256):
-                acc[:, way * half + c : way * half + c + 256] += jnp.dot(
-                    lhs, wbuf[s, way, :, c : c + 256], preferred_element_type=f32
+    def project(ring, acc, slots, fresh=False):
+        total_cols = acc.shape[1]
+        for slot in slots:
+            ring.need(slot)
+        for c in range(0, total_cols, 256):
+            total = None
+            for slot in slots:
+                at = pl.multiple_of(owner_of(slot) * kdim, kdim)
+                term = jnp.dot(
+                    norm[:, pl.ds(at, kdim)], ring.buf[slot, :, c : c + 256],
+                    preferred_element_type=f32,
                 )
-
-    start = max(mid, 1)
-
-    def body(s, carry):
-        @pl.when(s > start)
-        def _():
-            forward(s)
-
-        @pl.when(s == max(n - 2, start))
-        def _():
-            o_forward(0)
-
-        project(s)
-
-        @pl.when(s - start < start)
-        def _():
-            project(s - start)
-
-        return carry
-
-    lax.fori_loop(start, n, body, 0)
+                total = term if total is None else total + term
+            if fresh:
+                acc[:, c : c + 256] = total
+            else:
+                acc[:, c : c + 256] += total
+
+    def pairs_of():
+        return [(k, n - k) for k in range(1, n_half)]
+
+    project(ring_s, acc_s, (0,), True)
+    for pair in pairs_of():
+        project(ring_s, acc_s, pair)
+    early = min(2, PIECES_R)
+    pump(early)
+    project(ring_s, acc_s, (n_half,))
 
     def column(ref):
         index = lax.broadcasted_iota(jnp.int32, (heads, 1), 0)
@@ -307,7 +345,8 @@
             full = jnp.where(index == h, ref[h], full)
         return full
 
-    step = jax.nn.softplus(jnp.dot(norm[HALO:, :], step_w[...], preferred_element_type=f32).T + column(bias))
+    landed("v")
+    step = jax.nn.softplus(nt(step_w[...], norm[HALO:, :]) + column(bias))
     logs = -step * jnp.exp(column(rate)) + spikes[...]
     r_id = lax.broadcasted_iota(jnp.int32, (CHUNK, CHUNK), 0)
     c_id = lax.broadcasted_iota(jnp.int32, (CHUNK, CHUNK), 1)
@@ -333,24 +372,25 @@
     blocks = length // CHUNK
     running = jnp.zeros((STATE, heads_width), f32)
     before = jnp.zeros((1, heads_width), f32)
-    at_outer, at_inner, at_value, at_ogate, at_state = (i * cdim for i in range(5))
-    at_write = 5 * cdim
-    at_read = at_write + STATE
+    at_ogate, at_outer, at_inner, at_value = (i * cdim for i in range(4))
+    at_state, at_write, at_read = 0, cdim, cdim + STATE
+
+    def spans(b):
+        t0 = b * CHUNK
+        return (
+            slice(t0, t0 + CHUNK),
+            slice(t0 + HALO, t0 + HALO + CHUNK),
+            slice(t0 + HALO - 8, t0 + HALO + CHUNK),
+        )
+
+    def field(acc, begin, size, span):
+        return acc[span, begin : begin + size].astype(bf16).astype(f32)
+
     for b in range(blocks):
-        t0 = b * CHUNK
-        take = slice(t0 + HALO - 8, t0 + HALO + CHUNK)
-        own = slice(t0 + HALO, t0 + HALO + CHUNK)
-
-        def field(begin, size, span):
-            return acc[span, begin : begin + size].astype(bf16).astype(f32)
-
-        product = field(at_inner, cdim, take) * field(at_value, cdim, take)
-        mix = field(at_outer, cdim, own) * taps(product, taps_conv)
-        apart[t0 : t0 + CHUNK, 0:cdim] = mix.astype(bf16)
-        xs = silu(taps(field(at_state, cdim, take), taps_in))
-        wr = silu(taps(field(at_write, STATE, take), taps_wr))
-        rd = silu(taps(field(at_read, STATE, take), taps_rd))
-        span = slice(t0, t0 + CHUNK)
+        span, own, take = spans(b)
+        xs = silu(taps(field(acc_s, at_state, cdim, take), taps_in))
+        wr = silu(taps(field(acc_s, at_write, STATE, take), taps_wr))
+        rd = silu(taps(field(acc_s, at_read, STATE, take), taps_rd))
         cum = nt(lower, logs[:, span], highest)
         steps = nt(eye, step[:, span], highest)
         cum_wide = spread(cum)
@@ -367,6 +407,7 @@
             wr.T.astype(bf16), scaled, preferred_element_type=f32
         )
         before = before + last
+        pump(1)
     st_send[0:STATE, :] = running.astype(bf16)
     st_send[STATE:, :] = jnp.broadcast_to(jnp.exp(before), (HALO, heads_width)).astype(bf16)
 
@@ -395,11 +436,9 @@
         )
 
     x_copy().start()
-    o_next = 1
 
     def within(b):
-        t0 = b * CHUNK
-        span = slice(t0, t0 + CHUNK)
+        span, _, _ = spans(b)
         scores = nt(rdbuf[span, :], wrbuf[span, :])
         cum_t = lax.dot_general(
             logs[:, span], lower, (((1,), (1,)), ((), ())),
@@ -420,10 +459,9 @@
             ybuf[span, pair : pair + 128] = jnp.where(first, both[0], both[1])
 
     for b in range(blocks):
-        if b % 2 == 0 and o_next < n:
-            o_forward(o_next)
-            o_next += 1
         within(b)
+        if b % 2 == 1:
+            pump(1)
     x_copy().wait_recv()
     other = st_recv[0:STATE, :].astype(f32)
     other_decay = st_recv[STATE : STATE + 1, :].astype(f32)
@@ -436,6 +474,36 @@
     pair_decay = own_decay * other_decay
     first_decay = jnp.where(is_second, other_decay, jnp.ones_like(other_decay))
 
+    def link(j):
+        @pl.when(z == j)
+        def _():
+            if j == 0:
+                pair_buf[2] = jnp.zeros_like(pair_buf[2])
+            else:
+                e_copy().wait_recv()
+                pair_buf[2] = e_recv[...].astype(f32)
+            if j < depth - 1:
+                e_send[...] = (pair_buf[2] * pair_decay + pair_buf[0]).astype(bf16)
+                e_copy().start()
+
+    link(0)
+    project(ring_r, acc_r, (0,), True)
+    landed("o")
+    for k, pair in enumerate(pairs_of()):
+        if k < n_half - 2:
+            pump(PIECES_R // 2)
+            project(ring_r, acc_r, pair)
+            link(k + 1)
+            pump(PIECES_R // 2)
+        else:
+            pump(len(r_list))
+            for q in range(PIECES_O):
+                ring_o.forward(0, q)
+            o_list += ring_o.order(1)
+            project(ring_r, acc_r, pair)
+            for j in range(k + 1, depth):
+                link(j)
+
     group = (
         lax.div(lax.broadcasted_iota(jnp.int32, (heads_width, heads_width), 0), HEAD_DIM)
         == lax.div(lax.broadcasted_iota(jnp.int32, (heads_width, heads_width), 1), HEAD_DIM)
@@ -444,35 +512,38 @@
     for h in range(1, heads):
         direct_wide = jnp.where(lane >= h * HEAD_DIM, direct[h], direct_wide)
 
-    def finish():
-        before = jnp.zeros((1, heads_width), f32)
-        arriving = pair_buf[1] + first_decay * pair_buf[2]
-        for b in range(blocks):
-            t0 = b * CHUNK
-            span = slice(t0, t0 + CHUNK)
-            own = slice(t0 + HALO, t0 + HALO + CHUNK)
-            cum_wide = cumbuf[span, :]
-            entering = (stbuf[b] + jnp.exp(before) * arriving).astype(bf16)
-            before = before + cum_wide[CHUNK - 1 : CHUNK]
-            head_out = (
-                ybuf[span, :]
-                + jnp.dot(rdbuf[span, :], entering, preferred_element_type=f32) * jnp.exp(cum_wide)
-                + direct_wide * xbuf[span, :]
-            )
-            og = acc[own, at_ogate : at_ogate + cdim].astype(bf16).astype(f32)
-            gated = head_out * silu(og)
-            square = jnp.dot((gated * gated).astype(bf16), group, preferred_element_type=f32)
-            normalized = gated * lax.rsqrt(square * (1.0 / HEAD_DIM) + epsilon)
-            apart[span, cdim:] = (normalized * hscale[...].astype(f32).reshape(1, heads_width)).astype(bf16)
-
-    Y = T // CORES
-    core = lax.rem(tp, CORES)
-    chip = lax.div(tp, CORES)
-    partner = chip * CORES + 1 - core
-    ocols = 2 * ohalf
+    arriving = pair_buf[1] + first_decay * pair_buf[2]
+    so_far = jnp.zeros((1, heads_width), f32)
+    for b in range(blocks):
+        span, _, _ = spans(b)
+        cum_wide = cumbuf[span, :]
+        entering = (stbuf[b] + jnp.exp(so_far) * arriving).astype(bf16)
+        so_far = so_far + cum_wide[CHUNK - 1 : CHUNK]
+        ybuf[span, :] = (
+            ybuf[span, :]
+            + jnp.dot(rdbuf[span, :], entering, preferred_element_type=f32) * jnp.exp(cum_wide)
+            + direct_wide * xbuf[span, :]
+        )
+
+    project(ring_r, acc_r, (n_half,))
+
+    for b in range(blocks):
+        span, own, take = spans(b)
+        product = field(acc_r, at_inner, cdim, take) * field(acc_r, at_value, cdim, take)
+        mix = field(acc_r, at_outer, cdim, own) * taps(product, taps_conv)
+        apart[span, 0:cdim] = mix.astype(bf16)
+        gated = ybuf[span, :] * silu(field(acc_r, at_ogate, cdim, own))
+        square = jnp.dot((gated * gated).astype(bf16), group, preferred_element_type=f32)
+        normalized = gated * lax.rsqrt(square * (1.0 / HEAD_DIM) + epsilon)
+        apart[span, cdim:] = (
+            normalized * hscale[...].astype(f32).reshape(1, heads_width)
+        ).astype(bf16)
 
     def block_rows(y, c):
         return pl.ds(pl.multiple_of((y * CORES + c) * rows, rows), rows)
+
+    def columns_of(slot):
+        return pl.ds(pl.multiple_of(owner_of(slot) * ocols, ocols), ocols)
 
     def r1_copy(d, s):
         return pltpu.make_async_remote_copy(
@@ -486,104 +557,66 @@
 
     def r2_copy(d, s):
         return pltpu.make_async_remote_copy(
-            src_ref=p2.at[d, s],
-            dst_ref=r2.at[d, s],
+            src_ref=p2.at[d - 1, s],
+            dst_ref=far.at[d - 1, :, columns_of(s)],
             send_sem=r2s_sem.at[d, s],
             recv_sem=r2r_sem.at[d, s],
             device_id={"tp": lax.rem(chip + d, Y) * CORES + core},
             device_id_type=MESH,
         )
 
-    def reduce_far(s):
+    def near_copy(s):
+        return pltpu.make_async_copy(nbuf.at[s], near.at[:, columns_of(s)], near_sem.at[s])
+
+    def project_out(s):
+        ring_o.need(s)
+        part[s] = jnp.dot(apart[...], obuf[s], preferred_element_type=f32).astype(bf16)
+        for d in range(1, Y):
+            r1_copy(d, s).start()
+        r1_copy(0, s).start()
+
+    def reduce(s):
         for d in range(1, Y):
             r1_copy(d, s).wait_recv()
             mine = part[s, block_rows(lax.rem(chip + d, Y), core), :]
-            p2[d, s] = (mine.astype(f32) + r1[d, s].astype(f32)).astype(bf16)
+            p2[d - 1, s] = (mine.astype(f32) + r1[d, s].astype(f32)).astype(bf16)
             r2_copy(d, s).start()
-
-    def project_out(s, carry):
-        for way in range(2):
-            part[s, :, way * ohalf : (way + 1) * ohalf] = jnp.dot(
-                apart[...], obuf[s, way], preferred_element_type=f32
-            ).astype(bf16)
+        r1_copy(0, s).wait_recv()
+        mine = part[s, block_rows(chip, core), :]
+        nbuf[s] = (mine.astype(f32) + r1[0, s].astype(f32)).astype(bf16)
+        near_copy(s).start()
+
+    order = [0]
+    for pair in pairs_of():
+        order += list(pair)
+    order.append(n_half)
+    previous = None
+    for i, slot in enumerate(order):
+        if slot and slot < n_half:
+            pump(PIECES_O)
+        project_out(slot)
+        if previous is not None:
+            reduce(previous)
+        previous = slot
+    reduce(previous)
+
+    ring_s.drain()
+    ring_r.drain()
+    ring_o.drain()
+    for q in range(PIECES_T):
+        for d in range(Y):
+            t_copy(d, q).wait_send()
         for d in range(1, Y):
-            r1_copy(d, s).start()
-        r1_copy(0, s).start()
-
-        @pl.when(s > 0)
-        def _():
-            reduce_far(s - 1)
-
-        return carry
-
-    def link(j, carry):
-        @pl.when(z == j)
-        def _():
-            @pl.when(j == 0)
-            def _():
-                pair_buf[2] = jnp.zeros_like(pair_buf[2])
-
-            @pl.when(j > 0)
-            def _():
-                e_copy().wait_recv()
-                pair_buf[2] = e_recv[...].astype(f32)
-
-            @pl.when(j < depth - 1)
-            def _():
-                e_send[...] = (pair_buf[2] * pair_decay + pair_buf[0]).astype(bf16)
-                e_copy().start()
-
-            finish()
-            lax.fori_loop(0, o_next + j, project_out, 0)
-
-        @pl.when(o_next + j < n)
-        def _():
-            o_forward(o_next + j)
-
-            @pl.when(z <= j)
-            def _():
-                project_out(o_next + j, 0)
-
-        return carry
-
-    lax.fori_loop(0, depth, link, 0)
-
-    def rest(s, carry):
-        o_forward(s)
-        project_out(s, 0)
-        return carry
-
-    lax.fori_loop(min(o_next + depth, n), n, rest, 0)
-    reduce_far(n - 1)
-
-    def collect(s, carry):
-        r1_copy(0, s).wait_recv()
-        total = part[s, block_rows(chip, core), :].astype(f32) + r1[0, s].astype(f32)
-        for d in range(1, Y):
-            r2_copy(d, s).wait_recv()
-            total = total + r2[d, s].astype(f32)
-        for way in range(2):
-            at = pl.multiple_of(owner_of(s, way) * ocols + way * ohalf, ohalf)
-            out[:, pl.ds(at, ohalf)] = total[:, way * ohalf : (way + 1) * ohalf].astype(bf16)
-        return carry
-
-    lax.fori_loop(0, n, collect, 0)
-
-    def w_drain(s, carry):
-        for way in range(2):
-            for q in range(QIN):
-                w_copy(s, q, way).wait_send()
-            for q in range(QOUT):
-                o_copy(s, q, way).wait_send()
-        return carry
-
-    lax.fori_loop(0, n - 1, w_drain, 0)
-    for d in range(1, T):
-        t_copy(d).wait_send()
-
-    @pl.when(sp < n - 1)
+            u_copy(d, q).wait_send()
+
+    @pl.when(last_tp & (sp < n - 1))
     def _():
         h_copy().wait_send()
+
+    @pl.when(last_tp & (sp > 0))
+    def _():
+        for d in range(T - 1):
+            g_copy(d).wait_send()
 
     x_copy().wait_send()
 
@@ -591,14 +624,15 @@
     def _():
         e_copy().wait_send()
 
-    def r_drain(s, carry):
+    for s in range(n):
         for d in range(Y):
             r1_copy(d, s).wait_send()
         for d in range(1, Y):
             r2_copy(d, s).wait_send()
-        return carry
-
-    lax.fori_loop(0, n, r_drain, 0)
+        near_copy(s).wait()
+    for s in order:
+        for d in range(1, Y):
+            r2_copy(d, s).wait_recv()
 
 
 def shifted(shard, axis, by):
@@ -819,10 +853,13 @@
     kdim, cdim = outer_gate_weight.shape
     heads = step_size_bias.shape[0]
     hw = heads * HEAD_DIM
-    half = 3 * cdim
     length = rows * T
     ocols = conv_output_weight.shape[1]
-    if kdim % 128 or ocols % 256 or n % 2 or T % CORES or write_key_weight.shape[1] != STATE:
+    if (
+        kdim % 128 or ocols % 256 or n % 2 or n < 4 or n > 16 or T % CORES
+        or T < 2 * CORES
+        or write_key_weight.shape[1] != STATE
+    ):
         return plain_path(
             tokens, input_norm_scale, outer_gate_weight, inner_gate_weight,
             value_weight_matrix, output_gate_weight, state_input_weight, write_key_weight,
@@ -831,20 +868,39 @@
             direct_path_weight, head_norm_scale, conv_output_weight, state_output_weight,
         )
     Y = T // CORES
-    vm = pl.BlockSpec(memory_space=pltpu.VMEM)
     sm = pl.BlockSpec(memory_space=pltpu.SMEM)
     hbm = pl.BlockSpec(memory_space=pl.ANY)
     dma = pltpu.SemaphoreType.DMA
-    return pl.pallas_call(
+    s_cols, r_cols = cdim + 2 * STATE, 4 * cdim
+
+    def like(array):
+        return pltpu.VMEM(array.shape, array.dtype)
+
+    step_t = step_size_weight.T
+    near, far = pl.pallas_call(
         functools.partial(kernel, n, T),
-        out_shape=jax.ShapeDtypeStruct((rows, width), bf16),
-        in_specs=[vm] * 2 + [hbm] * 7 + [vm] * 5 + [sm] * 2 + [vm, sm, vm] + [hbm] * 2,
-        out_specs=vm,
+        out_shape=(
+            jax.ShapeDtypeStruct((rows, width), bf16),
+            jax.ShapeDtypeStruct((Y - 1, rows, width), bf16),
+        ),
+        in_specs=[hbm] * 14 + [sm] * 2 + [hbm, sm, hbm] + [hbm] * 2,
+        out_specs=(hbm, hbm),
         scratch_shapes=[
-            pltpu.VMEM((n, 2, kdim, half), bf16),
-            pltpu.VMEM((n, 2, cdim + hw, ocols // 2), bf16),
+            like(tokens),
+            like(input_norm_scale),
+            like(step_t),
+            like(gated_conv_weight),
+            like(input_conv_weight),
+            like(write_conv_weight),
+            like(read_conv_weight),
+            like(decay_spikes),
+            like(head_norm_scale),
+            pltpu.VMEM((n, kdim, s_cols), bf16),
+            pltpu.VMEM((n, kdim, r_cols), bf16),
+            pltpu.VMEM((n, cdim + hw, ocols), bf16),
             pltpu.VMEM((HALO + length, width), bf16),
-            pltpu.VMEM((HALO + length, 2 * half), f32),
+            pltpu.VMEM((HALO + length, s_cols), f32),
+            pltpu.VMEM((HALO + length, r_cols), f32),
             pltpu.VMEM((length, hw), bf16),
             pltpu.VMEM((length, hw), f32),
             pltpu.VMEM((length, STATE), bf16),
@@ -860,22 +916,28 @@
             pltpu.VMEM((length, cdim + hw), bf16),
             pltpu.VMEM((n, length, ocols), bf16),
             pltpu.VMEM((Y, n, rows, ocols), bf16),
-            pltpu.VMEM((Y, n, rows, ocols), bf16),
-            pltpu.VMEM((Y, n, rows, ocols), bf16),
-            dma((11,)),
-            dma((n, QIN, 2)),
-            dma((n, QIN, 2)),
-            dma((n, QOUT, 2)),
-            dma((n, QOUT, 2)),
-            dma((T,)),
-            dma((T,)),
+            pltpu.VMEM((Y - 1, n, rows, ocols), bf16),
+            pltpu.VMEM((n, rows, ocols), bf16),
+            dma((18,)),
+            dma((n // 2, PIECES_S, 2)),
+            dma((n // 2, PIECES_S, 2)),
+            dma((n // 2, PIECES_R, 2)),
+            dma((n // 2, PIECES_R, 2)),
+            dma((n // 2, PIECES_O, 2)),
+            dma((n // 2, PIECES_O, 2)),
+            dma((Y, PIECES_T)),
+            dma((Y, PIECES_T)),
+            dma((Y, PIECES_T)),
+            dma((Y, PIECES_T)),
             dma((2,)),
+            dma((2, T)),
             dma((2,)),
             dma((2,)),
             dma((Y, n)),
             dma((Y, n)),
             dma((Y, n)),
             dma((Y, n)),
+            dma((n,)),
         ],
         compiler_params=pltpu.CompilerParams(
             collective_id=0, has_side_effects=True, vmem_limit_bytes=62 * 1024 * 1024
@@ -883,11 +945,15 @@
     )(
         tokens, input_norm_scale, outer_gate_weight, inner_gate_weight,
         value_weight_matrix, output_gate_weight, state_input_weight, write_key_weight,
-        read_key_weight, step_size_weight, gated_conv_weight, input_conv_weight, write_conv_weight,
+        read_key_weight, step_t, gated_conv_weight, input_conv_weight, write_conv_weight,
         read_conv_weight, step_size_bias, log_decay_rate, decay_spikes, direct_path_weight,
         head_norm_scale,
         conv_output_weight, state_output_weight,
     )
+    total = near.astype(f32)
+    for d in range(Y - 1):
+        total = total + far[d].astype(f32)
+    return total.astype(bf16)
 
 
 def solution(mesh):

time: 113 us -> 100 us (0.88)
  Pallas kernels: 109 us -> 97.9 us
  local copies, waits for them, and re-layouts: 3.65 us -> 0 us
  other arithmetic: 0 us -> 2.12 us
    pallas_call x1, Pallas kernels: 109 us -> 97.9 us  [per_device(): pl.pallas_call(functools.partial(kernel, n, T), out_shape=(jax.ShapeDtype...]
    unnamed x2 -> x0, local copies, waits for them, and re-layouts: 3.65 us -> none
    convert_element_type x0 -> x1, other arithmetic: none -> 2.12 us  [per_device(): return total.astype(bf16)]
where the time goes in v1:
time: 100 us
  Pallas kernels  97.9 us (98%)
  other arithmetic  2.12 us (2%)
    pallas_call x1, Pallas kernels, per_device(): pl.pallas_call(functools.partial(kernel, n, T), out_shape=(jax.ShapeDtype...  97.9 us
    convert_element_type x1, other arithmetic, per_device(): return total.astype(bf16)  2.12 us

profile of v1, /device:TPU:0, one launch (start us, length us, event | category | flops | bytes accessed | tf_op | source)
XLA Modules:
  0.0 100.0 jit_solution(9116041319978148311)
XLA Ops:
  0.0 97.9 %shard_map.199 = (bf16[128,2048]{1,0:T(8,128)(2,1)}, bf16[1,128,2048]{2,1,0:T(8,128)(2,1)}) custom-call(bf16[128,2048]{1,0:T(8,128)(2,1)} %tokens_h.1, bf16[2048]{0:T(1024)(128)(2,1)} %in_scale_h.1, bf16[256,256]{1,0:T(8,128)(2,1)} %w_outer.1, bf16[256,256]{1,0:T(8,128)(2,1)} %w_inner.1, bf16[256,256]{1,0:T(8,128)(2,1)} %w_value.1, ...), custom_call_target="tpu_custom_call" | custom-call | tf_op jit(solution)/shard_map/pallas_call | solution.py:880
  97.9 2.1 %fusion = bf16[128,2048]{1,0:T(8,128)(2,1)} fusion(bf16[128,2048]{1,0:T(8,128)(2,1)} %get-tuple-element.7, bf16[1,128,2048]{2,1,0:T(8,128)(2,1)} %get-tuple-element.8), kind=kLoop, calls=%fused_computation.1 | loop fusion | flops 1048576 | bytes 1572864 | tf_op jit(solution)/shard_map/convert_element_type | solution.py:956

commit v2 on v1

--- a/solution.py
+++ b/solution.py
@@ -48,11 +48,15 @@
         return pltpu.make_async_remote_copy(
             src_ref=self.buf.at[src, cut],
             dst_ref=self.buf.at[dst, cut],
-            send_sem=self.send_sem.at[s, q, way],
-            recv_sem=self.recv_sem.at[s, q, way],
+            send_sem=self.send_sem,
+            recv_sem=self.recv_sem.at[self.flat(s, q, way)],
             device_id={"sp": self.neighbour[way]},
             device_id_type=MESH,
         )
+
+    def flat(self, s, q, way):
+        last = self.n // 2 - 1
+        return (s * self.pieces + q) * 2 + way if s < last else last * self.pieces * 2 + q
 
     def ways(self, s, q):
         if s < self.n // 2 - 1:
@@ -84,9 +88,15 @@
         return [(s, q) for s in range(first, self.n // 2) for q in range(self.pieces)]
 
     def drain(self):
-        for s, q in self.order(0):
-            for way in self.ways(s, q):
-                self.copy(s, q, way).wait_send()
+        every = self.buf.at[pl.ds(0, self.n - 1)]
+        pltpu.make_async_remote_copy(
+            src_ref=every,
+            dst_ref=every,
+            send_sem=self.send_sem,
+            recv_sem=self.recv_sem.at[0],
+            device_id={"sp": self.neighbour[0]},
+            device_id_type=MESH,
+        ).wait_send()
 
 
 def kernel(
@@ -146,12 +156,19 @@
         ],
         "o": pack((o_conv, o_state), obuf, True),
     }
+    whole = {"s": sbuf.at[0], "r": rbuf.at[0], "o": obuf.at[0]}
     local, index = {}, 0
     for name, pairs in groups.items():
         local[name] = []
         for src, dst in pairs:
-            local[name].append(pltpu.make_async_copy(src, dst, loc_sem.at[index]))
-            local[name][-1].start()
+            pltpu.make_async_copy(src, dst, loc_sem.at[index]).start()
+            if name not in whole:
+                local[name].append(pltpu.make_async_copy(src, dst, loc_sem.at[index]))
+                index += 1
+        if name in whole:
+            local[name].append(
+                pltpu.make_async_copy(whole[name], whole[name], loc_sem.at[index])
+            )
             index += 1
 
     def landed(name):
@@ -191,7 +208,7 @@
         return pltpu.make_async_remote_copy(
             src_ref=at_rows(tp, q),
             dst_ref=at_rows(tp, q),
-            send_sem=ts_sem.at[d, q],
+            send_sem=ts_sem,
             recv_sem=tr_sem.at[d, q],
             device_id={"tp": device},
             device_id_type=MESH,
@@ -202,7 +219,7 @@
         return pltpu.make_async_remote_copy(
             src_ref=at_rows(block, q),
             dst_ref=at_rows(block, q),
-            send_sem=us_sem.at[d, q],
+            send_sem=us_sem,
             recv_sem=ur_sem.at[d, q],
             device_id={"tp": partner},
             device_id_type=MESH,
@@ -222,8 +239,8 @@
         return pltpu.make_async_remote_copy(
             src_ref=norm.at[pl.ds(0, HALO)],
             dst_ref=norm.at[pl.ds(0, HALO)],
-            send_sem=g_sem.at[0, d],
-            recv_sem=g_sem.at[1, d],
+            send_sem=g_sem.at[0],
+            recv_sem=g_sem.at[1],
             device_id={"tp": d},
             device_id_type=MESH,
         )
@@ -295,7 +312,7 @@
             pltpu.make_async_remote_copy(
                 src_ref=at_rows(lax.rem(chip + Y - d, Y) * CORES + 1 - core, q),
                 dst_ref=at_rows(lax.rem(chip + Y - d, Y) * CORES + 1 - core, q),
-                send_sem=us_sem.at[d, q],
+                send_sem=us_sem,
                 recv_sem=ur_sem.at[d, q],
                 device_id={"tp": partner},
                 device_id_type=MESH,
@@ -407,7 +424,6 @@
             wr.T.astype(bf16), scaled, preferred_element_type=f32
         )
         before = before + last
-        pump(1)
     st_send[0:STATE, :] = running.astype(bf16)
     st_send[STATE:, :] = jnp.broadcast_to(jnp.exp(before), (HALO, heads_width)).astype(bf16)
 
@@ -436,6 +452,7 @@
         )
 
     x_copy().start()
+    pump(4)
 
     def within(b):
         span, _, _ = spans(b)
@@ -548,25 +565,34 @@
     def r1_copy(d, s):
         return pltpu.make_async_remote_copy(
             src_ref=part.at[s, block_rows(lax.rem(chip + d, Y), 1 - core)],
-            dst_ref=r1.at[d, s],
-            send_sem=r1s_sem.at[d, s],
-            recv_sem=r1r_sem.at[d, s],
+            dst_ref=r1.at[s, d],
+            send_sem=r1s_sem,
+            recv_sem=r1r_sem.at[s],
             device_id={"tp": partner},
             device_id_type=MESH,
         )
+
+    def bulk(ref, send, recv, device):
+        return pltpu.make_async_remote_copy(
+            src_ref=ref, dst_ref=ref, send_sem=send, recv_sem=recv, device_id={"tp": device},
+            device_id_type=MESH,
+        )
+
+    def r1_all(ref, recv):
+        return bulk(ref, r1s_sem, recv, partner)
 
     def r2_copy(d, s):
         return pltpu.make_async_remote_copy(
             src_ref=p2.at[d - 1, s],
             dst_ref=far.at[d - 1, :, columns_of(s)],
-            send_sem=r2s_sem.at[d, s],
-            recv_sem=r2r_sem.at[d, s],
+            send_sem=r2s_sem,
+            recv_sem=r2r_sem,
             device_id={"tp": lax.rem(chip + d, Y) * CORES + core},
             device_id_type=MESH,
         )
 
     def near_copy(s):
-        return pltpu.make_async_copy(nbuf.at[s], near.at[:, columns_of(s)], near_sem.at[s])
+        return pltpu.make_async_copy(nbuf.at[s], near.at[:, columns_of(s)], near_sem)
 
     def project_out(s):
         ring_o.need(s)
@@ -576,14 +602,13 @@
         r1_copy(0, s).start()
 
     def reduce(s):
+        r1_all(r1.at[s], r1r_sem.at[s]).wait_recv()
         for d in range(1, Y):
-            r1_copy(d, s).wait_recv()
             mine = part[s, block_rows(lax.rem(chip + d, Y), core), :]
-            p2[d - 1, s] = (mine.astype(f32) + r1[d, s].astype(f32)).astype(bf16)
+            p2[d - 1, s] = (mine.astype(f32) + r1[s, d].astype(f32)).astype(bf16)
             r2_copy(d, s).start()
-        r1_copy(0, s).wait_recv()
         mine = part[s, block_rows(chip, core), :]
-        nbuf[s] = (mine.astype(f32) + r1[0, s].astype(f32)).astype(bf16)
+        nbuf[s] = (mine.astype(f32) + r1[s, 0].astype(f32)).astype(bf16)
         near_copy(s).start()
 
     order = [0]
@@ -594,8 +619,10 @@
     for i, slot in enumerate(order):
         if slot and slot < n_half:
             pump(PIECES_O)
+        if slot == n_half:
+            reduce(previous)
         project_out(slot)
-        if previous is not None:
+        if slot != n_half and previous is not None:
             reduce(previous)
         previous = slot
     reduce(previous)
@@ -603,11 +630,8 @@
     ring_s.drain()
     ring_r.drain()
     ring_o.drain()
-    for q in range(PIECES_T):
-        for d in range(Y):
-            t_copy(d, q).wait_send()
-        for d in range(1, Y):
-            u_copy(d, q).wait_send()
+    bulk(norm.at[pl.ds(0, Y * rows)], ts_sem, tr_sem.at[0, 0], partner).wait_send()
+    bulk(norm.at[pl.ds(0, (Y - 1) * rows)], us_sem, ur_sem.at[0, 0], partner).wait_send()
 
     @pl.when(last_tp & (sp < n - 1))
     def _():
@@ -615,8 +639,7 @@
 
     @pl.when(last_tp & (sp > 0))
     def _():
-        for d in range(T - 1):
-            g_copy(d).wait_send()
+        bulk(norm.at[pl.ds(0, (T - 1) * HALO)], g_sem.at[0], g_sem.at[1], partner).wait_send()
 
     x_copy().wait_send()
 
@@ -624,15 +647,10 @@
     def _():
         e_copy().wait_send()
 
-    for s in range(n):
-        for d in range(Y):
-            r1_copy(d, s).wait_send()
-        for d in range(1, Y):
-            r2_copy(d, s).wait_send()
-        near_copy(s).wait()
-    for s in order:
-        for d in range(1, Y):
-            r2_copy(d, s).wait_recv()
+    r1_all(r1, r1r_sem.at[0]).wait_send()
+    bulk(p2, r2s_sem, r2r_sem, partner).wait_send()
+    pltpu.make_async_copy(far.at[0], near, near_sem).wait()
+    bulk(far, r2s_sem, r2r_sem, partner).wait_recv()
 
 
 def shifted(shard, axis, by):
@@ -915,29 +933,29 @@
             pltpu.VMEM((3, STATE, hw), f32),
             pltpu.VMEM((length, cdim + hw), bf16),
             pltpu.VMEM((n, length, ocols), bf16),
-            pltpu.VMEM((Y, n, rows, ocols), bf16),
+            pltpu.VMEM((n, Y, rows, ocols), bf16),
             pltpu.VMEM((Y - 1, n, rows, ocols), bf16),
             pltpu.VMEM((n, rows, ocols), bf16),
-            dma((18,)),
-            dma((n // 2, PIECES_S, 2)),
-            dma((n // 2, PIECES_S, 2)),
-            dma((n // 2, PIECES_R, 2)),
-            dma((n // 2, PIECES_R, 2)),
-            dma((n // 2, PIECES_O, 2)),
-            dma((n // 2, PIECES_O, 2)),
+            dma((12,)),
+            dma,
+            dma(((n - 1) * PIECES_S,)),
+            dma,
+            dma(((n - 1) * PIECES_R,)),
+            dma,
+            dma(((n - 1) * PIECES_O,)),
+            dma,
             dma((Y, PIECES_T)),
-            dma((Y, PIECES_T)),
-            dma((Y, PIECES_T)),
+            dma,
             dma((Y, PIECES_T)),
             dma((2,)),
-            dma((2, T)),
             dma((2,)),
             dma((2,)),
-            dma((Y, n)),
-            dma((Y, n)),
-            dma((Y, n)),
-            dma((Y, n)),
+            dma((2,)),
+            dma,
             dma((n,)),
+            dma,
+            dma,
+            dma,
         ],
         compiler_params=pltpu.CompilerParams(
             collective_id=0, has_side_effects=True, vmem_limit_bytes=62 * 1024 * 1024

time: 100 us -> 97.7 us (0.977)
  Pallas kernels: 97.9 us -> 95.4 us
    pallas_call x1, Pallas kernels: 97.9 us -> 95.4 us  [per_device(): pl.pallas_call(functools.partial(kernel, n, T), out_shape=(jax.ShapeDtype...]
where the time goes in v2:
time: 97.7 us; the launch traced here: 97.5 us
  Pallas kernels  95.4 us (98%)
  other arithmetic  2.12 us (2%)
    pallas_call x1, Pallas kernels, per_device(): pl.pallas_call(functools.partial(kernel, n, T), out_shape=(jax.ShapeDtype...  95.4 us
    convert_element_type x1, other arithmetic, per_device(): return total.astype(bf16)  2.12 us

profile of v2, /device:TPU:0, one launch (start us, length us, event | category | flops | bytes accessed | tf_op | source)
XLA Modules:
  0.0 97.5 jit_solution(9873603016205229860)
XLA Ops:
  0.0 95.4 %shard_map.199 = (bf16[128,2048]{1,0:T(8,128)(2,1)}, bf16[1,128,2048]{2,1,0:T(8,128)(2,1)}) custom-call(bf16[128,2048]{1,0:T(8,128)(2,1)} %tokens_h.1, bf16[2048]{0:T(1024)(128)(2,1)} %in_scale_h.1, bf16[256,256]{1,0:T(8,128)(2,1)} %w_outer.1, bf16[256,256]{1,0:T(8,128)(2,1)} %w_inner.1, bf16[256,256]{1,0:T(8,128)(2,1)} %w_value.1, ...), custom_call_target="tpu_custom_call" | custom-call | tf_op jit(solution)/shard_map/pallas_call | solution.py:898
  95.4 2.1 %fusion = bf16[128,2048]{1,0:T(8,128)(2,1)} fusion(bf16[128,2048]{1,0:T(8,128)(2,1)} %get-tuple-element.7, bf16[1,128,2048]{2,1,0:T(8,128)(2,1)} %get-tuple-element.8), kind=kLoop, calls=%fused_computation.1 | loop fusion | flops 1048576 | bytes 1572864 | tf_op jit(solution)/shard_map/convert_element_type | solution.py:974

commit v3 on v2

v3 whole, which is shorter than its diff:
```python
import functools

import jax
import jax.numpy as jnp
from jax import lax
from jax.experimental import pallas as pl
from jax.experimental.pallas import tpu as pltpu
from jax.sharding import PartitionSpec as P

HEAD_DIM = 64
STATE = 128
PLAIN_BLOCK = 64
CHUNK = 128
HALO = 16
PIECES_S = 4
PIECES_G = 2
PIECES_C = 4
PIECES_O = 2
PIECES_T = 2
PIECES_U = 4
PLANES = 4
CORES = 2
epsilon = 1e-05
highest = lax.Precision.HIGHEST
f32 = jnp.float32
bf16 = jnp.bfloat16
MESH = pl.DeviceIdType.MESH


def nt(a, b, precision=None):
    return lax.dot_general(
        a, b, (((1,), (1,)), ((), ())), preferred_element_type=f32, precision=precision
    )


def silu(v):
    return v / (1.0 + jnp.exp(-v))


def remote(src, dst, send, recv, device):
    return pltpu.make_async_remote_copy(
        src_ref=src, dst_ref=dst, send_sem=send, recv_sem=recv, device_id=device,
        device_id_type=MESH,
    )


class Slots:
    def __init__(self, buf, pieces, recv):
        self.buf, self.pieces, self.recv = buf, pieces, recv
        self.rows = buf.shape[1] // pieces
        self.waited = set()

    def piece(self, slot, q):
        return self.buf.at[slot, pl.ds(q * self.rows, self.rows)]

    def send(self, src, dst, q, sem, device):
        remote(
            self.piece(src, q), self.piece(dst, q), sem,
            self.recv.at[(dst - 1) * self.pieces + q], {"sp": device},
        ).start()

    def arrive(self, slot, q, sem, device):
        if (slot, q) not in self.waited:
            self.waited.add((slot, q))
            remote(
                self.piece(slot, q), self.piece(slot, q), sem,
                self.recv.at[(slot - 1) * self.pieces + q], {"sp": device},
            ).wait_recv()


def kernel(
    n,
    T,
    tokens_h, in_scale_h, w_outer, w_inner, w_value, w_ogate, w_state, w_write, w_read,
    step_w_h, taps_conv_h, taps_in_h, taps_wr_h, taps_rd_h,
    bias, rate, spikes_h, direct, hscale_h, o_conv, o_state,
    near, far,
    tokens, in_scale, step_w, taps_conv, taps_in, taps_wr, taps_rd, spikes, hscale,
    sbuf, gbuf, cbuf, obuf, norm, norm2, spikes2, acc_s, acc_g, acc_c,
    mixbuf, xbuf, wrbuf, rdbuf, ybuf, cumbuf, stbuf, runbuf, decbuf,
    st_send, st_recv, e_send, e_recv, mbuf, apart, part, r1, p2, nbuf,
    loc_sem, ss_sem, sr_sem, gs_sem, gr_sem, cs_sem, cr_sem, os_sem, ox_sem, or_sem,
    ts_sem, tr_sem, us_sem, ur_sem, vs_sem, vr_sem, t2s_sem, t2r_sem, u2s_sem, u2r_sem,
    h_sem, g_sem, k_sem, l_sem, x_sem, e_sem, ms_sem, mr_sem,
    r1s_sem, r1r_sem, r2s_sem, r2r_sem, near_sem,
):
    sp = lax.axis_index("sp")
    tp = lax.axis_index("tp")
    rows, width = tokens.shape
    kdim = w_outer.shape[0]
    cdim = w_outer.shape[1]
    length = rows * T
    heads_width = mbuf.shape[1]
    heads = heads_width // HEAD_DIM
    ocols = obuf.shape[2]
    Y = T // CORES

    barrier = pltpu.get_barrier_semaphore()
    for d in range(1, n):
        pl.semaphore_signal(
            barrier, inc=1, device_id={"sp": lax.rem(sp + d, n)}, device_id_type=MESH
        )
    for d in range(1, T):
        pl.semaphore_signal(
            barrier, inc=1, device_id={"tp": lax.rem(tp + d, T)}, device_id_type=MESH
        )

    def pack(refs, dst, rows_too=False):
        pairs, at = [], 0
        for ref in refs:
            if rows_too:
                pairs.append((ref, dst.at[0, pl.ds(at, ref.shape[0])]))
                at += ref.shape[0]
            else:
                pairs.append((ref, dst.at[0, :, pl.ds(at, ref.shape[1])]))
                at += ref.shape[1]
        return pairs

    groups = {
        "s": pack((w_state, w_write, w_read), sbuf),
        "t": [(tokens_h, tokens), (in_scale_h, in_scale)],
        "c": pack((w_outer, w_inner, w_value), cbuf),
        "g": pack((w_ogate,), gbuf),
        "v": [
            (spikes_h, spikes), (step_w_h, step_w), (taps_conv_h, taps_conv),
            (taps_in_h, taps_in), (taps_wr_h, taps_wr), (taps_rd_h, taps_rd), (hscale_h, hscale),
        ],
        "o": pack((o_conv, o_state), obuf, True),
    }
    whole = {"s": sbuf.at[0], "c": cbuf.at[0], "g": gbuf.at[0], "o": obuf.at[0]}
    local, index = {}, 0
    for name, pairs in groups.items():
        local[name] = []
        for src, dst in pairs:
            pltpu.make_async_copy(src, dst, loc_sem.at[index]).start()
            if name not in whole:
                local[name].append(pltpu.make_async_copy(src, dst, loc_sem.at[index]))
                index += 1
        if name in whole:
            local[name].append(
                pltpu.make_async_copy(whole[name], whole[name], loc_sem.at[index])
            )
            index += 1

    def landed(name):
        for copy in local[name]:
            copy.wait()

    z = lax.div(sp, 2)
    x = lax.rem(sp, 2)
    last_z = PLANES - 1
    odd_z = lax.rem(z, 2)
    pz = z + 1 - 2 * odd_z
    upper = lax.div(z, 2)
    inner_z = 1 + upper
    end_z = upper * last_z
    is_inner = z == inner_z
    inner = (1 - upper) * odd_z + upper * (1 - odd_z)
    mate = pz * 2 + x
    side = z * 2 + 1 - x
    cross = (last_z - z) * 2 + x
    beyond = inner * cross + (1 - inner) * side

    def pos_of(index):
        odd = lax.rem(index, 2)
        low = lax.div(index, 2)
        return (1 - odd) * low + odd * (n - 1 - low)

    def index_of(pos):
        high = lax.div(pos, n // 2)
        return (1 - high) * 2 * pos + high * (2 * (n - 1 - pos) + 1)

    pos = pos_of(sp)
    toward = pos_of(mate) - pos

    def plane_owner(slot):
        plane = (z, pz, last_z - inner_z, last_z - end_z)[slot % 4]
        return plane * 2 + (x if slot < 4 else 1 - x)

    def ring_slot(side_k, s):
        return n - 1 if s == n // 2 else 1 + side_k * (n // 2 - 1) + s - 1

    def ring_owner(slot):
        if slot == 0:
            return sp
        if slot == n - 1:
            return index_of(lax.rem(pos + n // 2, n))
        side_k, s = divmod(slot - 1, n // 2 - 1)
        way = toward if side_k == 0 else -toward
        return index_of(lax.rem(pos + n + way * (s + 1), n))

    link_device = (mate, beyond)

    class Ring:
        def __init__(self):
            self.rows = kdim // PIECES_C
            self.waited = set()

        def piece(self, slot, q):
            return cbuf.at[slot, pl.ds(q * self.rows, self.rows)]

        def has(self, link, s, q):
            return s < n // 2 - 1 or (q < PIECES_C // 2) == (link == 0)

        def copy(self, link, s, q):
            src = 0 if s == 0 else ring_slot(1 - link, s)
            dst = ring_slot(link, s + 1)
            return remote(
                self.piece(src, q), self.piece(dst, q), cs_sem,
                cr_sem.at[(dst - 1) * PIECES_C + q], {"sp": link_device[link]},
            )

        def arrive(self, slot, q):
            if (slot, q) not in self.waited:
                self.waited.add((slot, q))
                remote(
                    self.piece(slot, q), self.piece(slot, q), cs_sem,
                    cr_sem.at[(slot - 1) * PIECES_C + q], {"sp": mate},
                ).wait_recv()

        def forward(self, link, s, q):
            if s > 0:
                self.arrive(ring_slot(1 - link, s), q)
            self.copy(link, s, q).start()

        def need(self, slot):
            if slot:
                for q in range(PIECES_C):
                    self.arrive(slot, q)

    own_at = pl.multiple_of(HALO + tp * rows, HALO)
    core = lax.rem(tp, CORES)
    chip = lax.div(tp, CORES)
    partner = chip * CORES + 1 - core
    last_tp = tp == T - 1

    def spread_rows(ref, pieces, near_send, near_recv, far_send, far_recv):
        prow = rows // pieces

        def at_rows(block, q):
            return ref.at[pl.ds(pl.multiple_of(HALO + block * rows + q * prow, HALO), prow)]

        def first(d, q):
            device = partner if d == 0 else lax.rem(chip + d, Y) * CORES + core
            return remote(
                at_rows(tp, q), at_rows(tp, q), near_send, near_recv.at[d, q], {"tp": device}
            )

        def second(d, q, at_core):
            block = lax.rem(chip + Y - d, Y) * CORES + at_core
            return remote(
                at_rows(block, q), at_rows(block, q), far_send, far_recv.at[d, q],
                {"tp": partner},
            )

        def start(q):
            for d in range(1, Y):
                first(d, q).start()
            first(0, q).start()

        def relay(q):
            for d in range(1, Y):
                first(d, q).wait_recv()
                second(d, q, core).start()

        def finish():
            for q in range(pieces):
                first(0, q).wait_recv()
                for d in range(1, Y):
                    second(d, q, 1 - core).wait_recv()

        return at_rows, start, relay, finish

    _, t_start, t_relay, t_finish = spread_rows(norm, PIECES_T, ts_sem, tr_sem, us_sem, ur_sem)
    u_rows, u_start, u_relay, u_finish = spread_rows(
        norm2, PIECES_U, t2s_sem, t2r_sem, u2s_sem, u2r_sem
    )

    def v_copy(q):
        prow = rows // PIECES_U
        src = norm.at[pl.ds(pl.multiple_of(own_at + q * prow, HALO), prow)]
        return remote(src, u_rows(tp, q), vs_sem, vr_sem.at[q], {"sp": mate})

    def k_copy():
        cut = pl.ds(0, HALO)
        return remote(norm.at[cut], norm2.at[cut], k_sem.at[0], k_sem.at[1], {"sp": mate})

    def l_copy():
        return remote(spikes, spikes2, l_sem.at[0], l_sem.at[1], {"sp": mate})

    def h_copy():
        return remote(
            norm.at[pl.ds(length, HALO)], norm.at[pl.ds(0, HALO)], h_sem.at[0], h_sem.at[1],
            {"sp": lax.rem(sp + 1, n)},
        )

    def g_copy(d):
        cut = pl.ds(0, HALO)
        return remote(norm.at[cut], norm.at[cut], g_sem.at[0], g_sem.at[1], {"tp": d})

    def halo_relay():
        @pl.when(last_tp & (sp > 0))
        def _():
            h_copy().wait_recv()
            for d in range(T - 1):
                g_copy(d).start()

    def halo_ready():
        @pl.when((tp < T - 1) & (sp > 0))
        def _():
            g_copy(0).wait_recv()

        @pl.when(sp == 0)
        def _():
            norm[0:HALO, :] = jnp.zeros((HALO, width), bf16)

    def project(acc, source, buf, slots, owner, fresh=False):
        for c in range(0, acc.shape[1], 256):
            total = None
            for slot in slots:
                at = pl.multiple_of(owner(slot) * kdim, kdim)
                term = jnp.dot(
                    source[:, pl.ds(at, kdim)], buf[slot, :, c : c + 256],
                    preferred_element_type=f32,
                )
                total = term if total is None else total + term
            if fresh:
                acc[:, c : c + 256] = total
            else:
                acc[:, c : c + 256] += total

    def column(ref):
        index = lax.broadcasted_iota(jnp.int32, (heads, 1), 0)
        full = jnp.full((heads, 1), ref[0], f32)
        for h in range(1, heads):
            full = jnp.where(index == h, ref[h], full)
        return full

    lane = lax.broadcasted_iota(jnp.int32, (1, heads_width), 1)

    def spread(columns):
        full = jnp.broadcast_to(columns[:, 0:1], (columns.shape[0], heads_width))
        for h in range(1, heads):
            full = jnp.where(lane >= h * HEAD_DIM, columns[:, h : h + 1], full)
        return full

    def taps(u, weights):
        k_taps = weights.shape[0]
        w = weights[...].astype(f32)
        total = w[k_taps - 1 : k_taps] * u[8:]
        for k in range(k_taps - 1):
            total = total + w[k : k + 1] * pltpu.roll(u, k_taps - 1 - k, 0)[8:]
        return total

    blocks = length // CHUNK

    def spans(b):
        t0 = b * CHUNK
        return (
            slice(t0, t0 + CHUNK),
            slice(t0 + HALO, t0 + HALO + CHUNK),
            slice(t0 + HALO - 8, t0 + HALO + CHUNK),
        )

    def field(acc, begin, size, span):
        return acc[span, begin : begin + size].astype(bf16).astype(f32)

    def conv_step(ring, s):
        slots = (0,) if s == 0 else (n - 1,) if s == n // 2 else (ring_slot(0, s), ring_slot(1, s))
        for slot in slots:
            ring.need(slot)
        project(acc_c, norm, cbuf, slots, ring_owner, s == 0)

    def conv_mix():
        for b in range(blocks):
            span, own, take = spans(b)
            product = field(acc_c, cdim, cdim, take) * field(acc_c, 2 * cdim, cdim, take)
            mix = field(acc_c, 0, cdim, own) * taps(product, taps_conv)
            apart[span, 0:cdim] = mix.astype(bf16)

    def m_copy(b):
        cut = pl.ds(b * CHUNK, CHUNK)
        return remote(
            mbuf.at[cut], apart.at[cut, pl.ds(cdim, heads_width)], ms_sem, mr_sem.at[b],
            {"sp": mate},
        )

    def x_copy():
        return remote(st_send, st_recv, x_sem.at[0], x_sem.at[1], {"sp": side})

    def e_copy():
        return remote(e_send, e_recv, e_sem.at[0], e_sem.at[1], {"sp": cross})

    def inner_part():
        sl = Slots(sbuf, PIECES_S, sr_sem)
        gl = Slots(gbuf, PIECES_G, gr_sem)
        ol = Slots(obuf, PIECES_O, or_sem)
        ring = Ring()
        forwards = [(link, 1, q) for link in (0, 1) for q in range(PIECES_C)]
        step_two = sorted((q + 2.5 * link, link, q) for link in (0, 1) for q in range(PIECES_C))
        forwards += [(link, 2, q) for _, link, q in step_two]
        for q in range(PIECES_C // 2):
            forwards += [(0, 3, q), (1, 3, PIECES_C // 2 + q)]
        done = [0]

        def pump(count):
            for _ in range(count):
                if done[0] < len(forwards):
                    ring.forward(*forwards[done[0]])
                    done[0] += 1

        r_id = lax.broadcasted_iota(jnp.int32, (CHUNK, CHUNK), 0)
        c_id = lax.broadcasted_iota(jnp.int32, (CHUNK, CHUNK), 1)
        causal = r_id >= c_id
        lower = causal.astype(f32)
        eye = (r_id == c_id).astype(f32)

        for q in range(PIECES_C):
            ring.forward(0, 0, q)
        for q in range(PIECES_S):
            sl.arrive(1, q, ss_sem, mate)
            sl.send(1, 3, q, ss_sem, cross)
            sl.send(1, 5, q, ss_sem, side)
        for q in range(PIECES_S):
            sl.arrive(2, q, ss_sem, mate)
            sl.send(2, 6, q, ss_sem, side)
        for q in range(PIECES_C):
            ring.forward(1, 0, q)
        t_relay(0)
        landed("g")
        for q in range(PIECES_G):
            gl.send(0, 2, q, gs_sem, cross)
        landed("o")
        for q in range(PIECES_O):
            ol.send(0, 2, q, os_sem, cross)
            ol.send(0, 1, q, os_sem, mate)
        for q in range(PIECES_S):
            sl.arrive(3, q, ss_sem, mate)
            sl.send(3, 7, q, ss_sem, side)
        for q in range(PIECES_G):
            gl.send(0, 4, q, gs_sem, side)
        halo_relay()
        for q in range(PIECES_U):
            v_copy(q).wait_recv()
            u_start(q)
            if q == 0:
                for p in range(1, PIECES_T):
                    t_relay(p)
            if q > 0:
                pump(1)
                u_relay(q - 1)
        pump(1)
        t_finish()
        halo_ready()
        for q in range(PIECES_G):
            gl.arrive(1, q, gs_sem, mate)
            gl.send(1, 3, q, gs_sem, cross)
            gl.send(1, 5, q, gs_sem, side)
        u_relay(PIECES_U - 1)
        for slot in range(1, n):
            for q in range(PIECES_S):
                sl.arrive(slot, q, ss_sem, mate)
        project(acc_s.at[0], norm, sbuf, range(0, 4), plane_owner, True)
        project(acc_s.at[0], norm, sbuf, range(4, 8), plane_owner)
        for q in range(PIECES_G):
            gl.arrive(2, q, gs_sem, mate)
            gl.send(2, 6, q, gs_sem, side)
        k_copy().wait_recv()
        u_finish()
        project(acc_s.at[1], norm2, sbuf, range(0, 4), plane_owner, True)
        project(acc_s.at[1], norm2, sbuf, range(4, 8), plane_owner)
        pump(2)
        landed("v")
        l_copy().wait_recv()

        logs_of = []
        for k, (source, spike) in enumerate(((norm, spikes), (norm2, spikes2))):
            step = jax.nn.softplus(nt(step_w[...], source[HALO:, :]) + column(bias))
            logs = -step * jnp.exp(column(rate)) + spike[...]
            logs_of.append(logs)
            running = jnp.zeros((STATE, heads_width), f32)
            before = jnp.zeros((1, heads_width), f32)
            acc = acc_s.at[k]
            for b in range(blocks):
                span, own, take = spans(b)
                xs = silu(taps(field(acc, 0, cdim, take), taps_in))
                wr = silu(taps(field(acc, cdim, STATE, take), taps_wr))
                rd = silu(taps(field(acc, cdim + STATE, STATE, take), taps_rd))
                cum = nt(lower, logs[:, span], highest)
                steps = nt(eye, step[:, span], highest)
                cum_wide = spread(cum)
                weighted = xs * spread(steps)
                xbuf[k, span, :] = xs
                mixbuf[k, span, :] = weighted.astype(bf16)
                wrbuf[k, span, :] = wr.astype(bf16)
                rdbuf[k, span, :] = rd.astype(bf16)
                cumbuf[k, span, :] = cum_wide
                last = cum_wide[CHUNK - 1 : CHUNK]
                scaled = (weighted * jnp.exp(last - cum_wide)).astype(bf16)
                stbuf[k, b] = running
                running = running * jnp.exp(last) + jnp.dot(
                    wr.T.astype(bf16), scaled, preferred_element_type=f32
                )
                before = before + last
                if k == 0 and b % 2 == 1:
                    pump(1)
            runbuf[k] = running
            decbuf[k] = jnp.exp(before)
            st_send[k, 0:STATE, :] = running.astype(bf16)
            st_send[k, STATE:, :] = jnp.broadcast_to(
                jnp.exp(before), (HALO, heads_width)
            ).astype(bf16)
            if k == 0:
                for q in range(PIECES_O):
                    ol.arrive(2, q, os_sem, mate)
                    ol.send(2, 2, q, os_sem, mate)

        x_copy().start()
        for q in range(PIECES_G):
            gl.arrive(3, q, gs_sem, mate)
            gl.send(3, 7, q, gs_sem, side)

        def within(k, b):
            span, _, _ = spans(b)
            scores = nt(rdbuf[k, span, :], wrbuf[k, span, :])
            cum_t = lax.dot_general(
                logs_of[k][:, span], lower, (((1,), (1,)), ((), ())),
                preferred_element_type=f32, precision=highest,
            )
            for pair in range(0, heads_width, 128):
                both = []
                for h in range(pair // HEAD_DIM, (pair + 128) // HEAD_DIM):
                    diff = cumbuf[k, span, h * HEAD_DIM : h * HEAD_DIM + 1] - cum_t[h : h + 1, :]
                    damped = scores * jnp.exp(jnp.where(causal, diff, -1e30))
                    both.append(
                        jnp.dot(
                            damped.astype(bf16), mixbuf[k, span, pair : pair + 128],
                            preferred_element_type=f32,
                        )
                    )
                first = lax.broadcasted_iota(jnp.int32, (1, 128), 1) < HEAD_DIM
                ybuf[k, span, pair : pair + 128] = jnp.where(first, both[0], both[1])

        for b in range(blocks):
            within(1, b)
        pump(1)
        for slot in (0, 2):
            for q in range(PIECES_O):
                ol.send(slot, 4 + slot, q, ox_sem, side)
        for b in range(blocks):
            within(0, b)
        pump(1)
        x_copy().wait_recv()
        second = jnp.broadcast_to(x, (1, heads_width)) == 1
        pair, pair_decay, other, first_decay = [], [], [], []
        for k in range(2):
            theirs = st_recv[k, 0:STATE, :].astype(f32)
            their_decay = st_recv[k, STATE : STATE + 1, :].astype(f32)
            pair.append(
                jnp.where(
                    second, theirs * decbuf[k] + runbuf[k], runbuf[k] * their_decay + theirs
                )
            )
            pair_decay.append(decbuf[k] * their_decay)
            other.append(jnp.where(second, theirs, jnp.zeros_like(theirs)))
            first_decay.append(jnp.where(second, their_decay, jnp.ones_like(their_decay)))

        @pl.when(upper == 0)
        def _():
            e_send[...] = (pair[1] * pair_decay[0] + pair[0]).astype(bf16)
            e_copy().start()
            runbuf[1] = other[1]
            runbuf[0] = other[0] + first_decay[0] * pair[1]

        @pl.when(upper == 1)
        def _():
            runbuf[0] = other[0]
            runbuf[1] = other[1] + first_decay[1] * pair[0]
            decbuf[0] = first_decay[0]
            decbuf[1] = first_decay[1] * pair_decay[0]

        pump(2)
        for q in range(PIECES_O):
            ol.arrive(1, q, os_sem, mate)
            ol.send(1, 3, q, os_sem, cross)
            ol.send(1, 5, q, ox_sem, side)
        pump(1)
        for slot in range(1, n - 1):
            for q in range(PIECES_G):
                gl.arrive(slot, q, gs_sem, mate)
        for k, source in enumerate((norm, norm2)):
            project(acc_g.at[k], source, gbuf, range(n - 1), plane_owner, True)
            pump(1)
        conv_step(ring, 0)
        pump(1)
        for q in range(PIECES_G):
            gl.arrive(n - 1, q, gs_sem, mate)
        for k, source in enumerate((norm, norm2)):
            project(acc_g.at[k], source, gbuf, (n - 1,), plane_owner)

        @pl.when(upper == 1)
        def _():
            e_copy().wait_recv()
            entering = e_recv[...].astype(f32)
            for k in range(2):
                runbuf[k] = runbuf[k] + decbuf[k] * entering

        group = (
            lax.div(lax.broadcasted_iota(jnp.int32, (heads_width, heads_width), 0), HEAD_DIM)
            == lax.div(lax.broadcasted_iota(jnp.int32, (heads_width, heads_width), 1), HEAD_DIM)
        ).astype(bf16)
        direct_wide = jnp.full((1, heads_width), direct[0], f32)
        for h in range(1, heads):
            direct_wide = jnp.where(lane >= h * HEAD_DIM, direct[h], direct_wide)

        for k in (1, 0):
            so_far = jnp.zeros((1, heads_width), f32)
            for b in range(blocks):
                span, own, _ = spans(b)
                cum_wide = cumbuf[k, span, :]
                entering = (stbuf[k, b] + jnp.exp(so_far) * runbuf[k]).astype(bf16)
                so_far = so_far + cum_wide[CHUNK - 1 : CHUNK]
                head_out = (
                    ybuf[k, span, :]
                    + jnp.dot(rdbuf[k, span, :], entering, preferred_element_type=f32)
                    * jnp.exp(cum_wide)
                    + direct_wide * xbuf[k, span, :]
                )
                gated = head_out * silu(field(acc_g.at[k], 0, cdim, own))
                square = jnp.dot((gated * gated).astype(bf16), group, preferred_element_type=f32)
                normalized = gated * lax.rsqrt(square * (1.0 / HEAD_DIM) + epsilon)
                result = (
                    normalized * hscale[...].astype(f32).reshape(1, heads_width)
                ).astype(bf16)
                if k == 1:
                    mbuf[span, :] = result
                    m_copy(b).start()
                else:
                    apart[span, cdim:] = result
        pump(1)
        conv_step(ring, 1)
        pump(1)
        conv_step(ring, 2)
        pump(len(forwards))
        for q in range(PIECES_O):
            ol.arrive(3, q, os_sem, mate)
            ol.send(3, 3, q, os_sem, mate)
            ol.send(3, 7, q, ox_sem, side)
        conv_step(ring, 3)
        conv_step(ring, n // 2)
        conv_mix()

    def blocks_sent(buf, count, sem):
        every = buf.at[pl.ds(0, count)]
        remote(every, every, sem, cr_sem.at[0], {"sp": mate}).wait_send()

    def end_part():
        gl = Slots(gbuf, PIECES_G, gr_sem)
        ol = Slots(obuf, PIECES_O, or_sem)
        ring = Ring()
        for q in range(PIECES_U):
            v_copy(q).start()
        for q in range(PIECES_C):
            ring.forward(1, 0, q)
        landed("v")
        l_copy().start()
        landed("g")
        for q in range(PIECES_G):
            gl.send(0, 1, q, gs_sem, mate)
        t_relay(0)
        for q in range(PIECES_C):
            ring.forward(1, 1, q)
        for q in range(1, PIECES_T):
            t_relay(q)
        halo_relay()
        halo_ready()
        k_copy().start()
        landed("o")
        for q in range(PIECES_C):
            ring.forward(0, 0, q)
        for q in range(PIECES_O):
            ol.send(0, 1, q, os_sem, mate)
        for q in range(PIECES_O):
            ol.send(0, 4, q, ox_sem, side)
        for q in range(PIECES_C):
            ring.forward(0, 1, q)
        for q in range(PIECES_O):
            ol.arrive(1, q, os_sem, mate)
            ol.send(1, 5, q, ox_sem, side)
        for q in range(PIECES_C):
            ring.forward(0, 2, q)
        t_finish()
        conv_step(ring, 0)
        conv_step(ring, 1)
        for q in range(PIECES_C):
            ring.forward(1, 2, q)
        for q in range(PIECES_C // 2):
            ring.forward(0, 3, q)
        conv_step(ring, 2)
        for q in range(PIECES_O):
            ol.arrive(2, q, os_sem, mate)
            ol.send(2, 6, q, ox_sem, side)
        for q in range(PIECES_C // 2, PIECES_C):
            ring.forward(1, 3, q)
        conv_step(ring, 3)
        for q in range(PIECES_O):
            ol.arrive(3, q, os_sem, mate)
            ol.send(3, 7, q, ox_sem, side)
        conv_step(ring, n // 2)
        conv_mix()
        for b in range(blocks):
            m_copy(b).wait_recv()

    landed("s")
    pl.semaphore_wait(barrier, n - 1 + T - 1)
    first_s = Slots(sbuf, PIECES_S, sr_sem)

    @pl.when(is_inner)
    def _():
        for q in range(PIECES_S):
            first_s.send(0, 2, q, ss_sem, cross)
            first_s.send(0, 4, q, ss_sem, side)

    @pl.when(z == end_z)
    def _():
        for q in range(PIECES_S):
            first_s.send(0, 1, q, ss_sem, mate)

    landed("t")
    value = tokens[...].astype(f32)
    value = value * lax.rsqrt(jnp.mean(value * value, axis=1, keepdims=True) + epsilon)
    norm[pl.ds(own_at, rows), :] = (
        value * in_scale[...].astype(f32).reshape(1, width)
    ).astype(bf16)
    for q in range(PIECES_T):
        t_start(q)

    @pl.when(last_tp & (sp < n - 1))
    def _():
        h_copy().start()

    landed("c")

    @pl.when(is_inner)
    def _():
        inner_part()

    @pl.when(z == end_z)
    def _():
        end_part()

    def block_rows(y, c):
        return pl.ds(pl.multiple_of((y * CORES + c) * rows, rows), rows)

    def columns_of(slot):
        return pl.ds(pl.multiple_of(plane_owner(slot) * ocols, ocols), ocols)

    def r1_copy(d, s):
        return remote(
            part.at[s, block_rows(lax.rem(chip + d, Y), 1 - core)], r1.at[s, d], r1s_sem,
            r1r_sem.at[s], {"tp": partner},
        )

    def r2_copy(d, s):
        return remote(
            p2.at[d - 1, s], far.at[d - 1, :, columns_of(s)], r2s_sem, r2r_sem,
            {"tp": lax.rem(chip + d, Y) * CORES + core},
        )

    def near_copy(s):
        return pltpu.make_async_copy(nbuf.at[s], near.at[:, columns_of(s)], near_sem)

    o_last = Slots(obuf, PIECES_O, or_sem)

    def project_out(s):
        if s >= 4:
            for q in range(PIECES_O):
                o_last.arrive(s, q, os_sem, mate)
        part[s] = jnp.dot(apart[...], obuf[s], preferred_element_type=f32).astype(bf16)
        for d in range(1, Y):
            r1_copy(d, s).start()
        r1_copy(0, s).start()

    def reduce(s):
        remote(r1.at[s], r1.at[s], r1s_sem, r1r_sem.at[s], {"tp": partner}).wait_recv()
        for d in range(1, Y):
            mine = part[s, block_rows(lax.rem(chip + d, Y), core), :]
            p2[d - 1, s] = (mine.astype(f32) + r1[s, d].astype(f32)).astype(bf16)
            r2_copy(d, s).start()
        mine = part[s, block_rows(chip, core), :]
        nbuf[s] = (mine.astype(f32) + r1[s, 0].astype(f32)).astype(bf16)
        near_copy(s).start()

    order = [0, 1, 2, 4, 5, 6, 3, 7]
    previous = None
    for slot in order:
        if slot == order[-1]:
            reduce(previous)
        project_out(slot)
        if slot != order[-1] and previous is not None:
            reduce(previous)
        previous = slot
    reduce(previous)

    @pl.when(is_inner)
    def _():
        x_copy().wait_send()

        @pl.when(upper == 0)
        def _():
            e_copy().wait_send()

        blocks_sent(sbuf, 6, ss_sem)
        blocks_sent(gbuf, 6, gs_sem)
        blocks_sent(obuf, 5, os_sem)
        remote(mbuf, mbuf, ms_sem, mr_sem.at[0], {"sp": mate}).wait_send()
        remote(
            norm2.at[pl.ds(0, Y * rows)], norm2.at[pl.ds(0, Y * rows)], t2s_sem,
            t2r_sem.at[0, 0], {"tp": partner},
        ).wait_send()
        remote(
            norm2.at[pl.ds(0, (Y - 1) * rows)], norm2.at[pl.ds(0, (Y - 1) * rows)], u2s_sem,
            u2r_sem.at[0, 0], {"tp": partner},
        ).wait_send()

    @pl.when(z == end_z)
    def _():
        blocks_sent(sbuf, 1, ss_sem)
        blocks_sent(gbuf, 1, gs_sem)
        blocks_sent(obuf, 1, os_sem)
        remote(
            norm.at[pl.ds(0, rows)], norm.at[pl.ds(0, rows)], vs_sem, vr_sem.at[0], {"sp": mate}
        ).wait_send()
        k_copy().wait_send()
        l_copy().wait_send()

    blocks_sent(cbuf, n - 1, cs_sem)
    blocks_sent(obuf, 4, ox_sem)
    remote(
        norm.at[pl.ds(0, Y * rows)], norm.at[pl.ds(0, Y * rows)], ts_sem, tr_sem.at[0, 0],
        {"tp": partner},
    ).wait_send()
    remote(
        norm.at[pl.ds(0, (Y - 1) * rows)], norm.at[pl.ds(0, (Y - 1) * rows)], us_sem,
        ur_sem.at[0, 0], {"tp": partner},
    ).wait_send()

    @pl.when(last_tp & (sp < n - 1))
    def _():
        h_copy().wait_send()

    @pl.when(last_tp & (sp > 0))
    def _():
        cut = pl.ds(0, (T - 1) * HALO)
        remote(norm.at[cut], norm.at[cut], g_sem.at[0], g_sem.at[1], {"tp": partner}).wait_send()

    remote(r1, r1, r1s_sem, r1r_sem.at[0], {"tp": partner}).wait_send()
    remote(p2, p2, r2s_sem, r2r_sem, {"tp": partner}).wait_send()
    pltpu.make_async_copy(far.at[0], near, near_sem).wait()
    remote(far, far, r2s_sem, r2r_sem, {"tp": partner}).wait_recv()


def shifted(shard, axis, by):
    devices = lax.axis_size(axis)
    pairs = [(i, i + by) for i in range(devices) if 0 <= i + by < devices]
    return lax.ppermute(shard, axis, pairs)


def prefix(shard, axis, combine, identity):
    devices, index = (lax.axis_size(axis), lax.axis_index(axis))
    everything = jax.tree.map(
        lambda part, kind: lax.all_gather(part.astype(kind), axis),
        shard,
        (jnp.bfloat16, jnp.bfloat16),
    )
    start = jax.tree.map(
        lambda part, zero: jnp.broadcast_to(jnp.asarray(zero, part.dtype), part.shape),
        shard,
        identity,
    )

    def turn(k, before):
        reached = k < index
        new = combine(
            before, jax.tree.map(lambda part, own: part[k].astype(own.dtype), everything, shard)
        )
        return jax.tree.map(lambda a, b: jnp.where(reached, a, b), new, before)

    return lax.fori_loop(0, devices, turn, start)


def causal_taps(values, rim_rows, tap_weights):
    tap_count = tap_weights.shape[0]
    length = values.shape[0]
    padded = jnp.concatenate([rim_rows, values], axis=0)
    running = tap_weights[0] * padded[0:length]
    for offset in range(1, tap_count):
        running = running + tap_weights[offset] * padded[offset : offset + length]
    return running


def combine_states(earlier, later):
    return (earlier[0] * later[0], earlier[1] * later[0][:, None, None] + later[1])


def plain_path(
    tokens,
    input_norm_scale,
    outer_gate_weight,
    inner_gate_weight,
    value_weight_matrix,
    output_gate_weight,
    state_input_weight,
    write_key_weight,
    read_key_weight,
    step_size_weight,
    gated_conv_weight,
    input_conv_weight,
    write_conv_weight,
    read_conv_weight,
    step_size_bias,
    log_decay_rate,
    decay_spikes,
    direct_path_weight,
    head_norm_scale,
    conv_output_weight,
    state_output_weight,
):
    token_rows = tokens.astype(jnp.float32)
    scaled = token_rows * lax.rsqrt(
        jnp.mean(token_rows * token_rows, axis=1, keepdims=True) + epsilon
    )
    normed_own = (scaled * input_norm_scale.astype(jnp.float32)).astype(jnp.bfloat16)
    normed = lax.all_gather(normed_own, "tp", axis=0, tiled=True)
    length = normed.shape[0]
    pieces = (
        lax.all_gather(outer_gate_weight, "sp", axis=0, tiled=True),
        lax.all_gather(inner_gate_weight, "sp", axis=0, tiled=True),
        lax.all_gather(value_weight_matrix, "sp", axis=0, tiled=True),
        lax.all_gather(output_gate_weight, "sp", axis=0, tiled=True),
        lax.all_gather(state_input_weight, "sp", axis=0, tiled=True),
        lax.all_gather(write_key_weight, "sp", axis=0, tiled=True),
        lax.all_gather(read_key_weight, "sp", axis=0, tiled=True),
    )
    projected = tuple(
        (jnp.dot(normed, weight_rows, preferred_element_type=jnp.float32) for weight_rows in pieces)
    )
    outer_gate, inner_gate, conv_input, out_gate, state_input, write_keys, read_keys = [
        member.astype(jnp.bfloat16) for member in projected
    ]
    step_raw = jnp.dot(normed, step_size_weight, preferred_element_type=jnp.float32)
    short_rim = gated_conv_weight.shape[0] - 1
    state_rim = input_conv_weight.shape[0] - 1
    rim_rows = shifted(
        (
            inner_gate[length - short_rim :],
            conv_input[length - short_rim :],
            state_input[length - state_rim :],
            write_keys[length - state_rim :],
            read_keys[length - state_rim :],
        ),
        "sp",
        1,
    )
    product = inner_gate.astype(jnp.float32) * conv_input.astype(jnp.float32)
    rim_product = rim_rows[0].astype(jnp.float32) * rim_rows[1].astype(jnp.float32)
    mixer_part = (
        outer_gate.astype(jnp.float32)
        * causal_taps(product, rim_product, gated_conv_weight.astype(jnp.float32))
    ).astype(jnp.bfloat16)
    seq_input = jax.nn.silu(
        causal_taps(
            state_input.astype(jnp.float32),
            rim_rows[2].astype(jnp.float32),
            input_conv_weight.astype(jnp.float32),
        )
    )
    seq_write = jax.nn.silu(
        causal_taps(
            write_keys.astype(jnp.float32),
            rim_rows[3].astype(jnp.float32),
            write_conv_weight.astype(jnp.float32),
        )
    )
    seq_read = jax.nn.silu(
        causal_taps(
            read_keys.astype(jnp.float32),
            rim_rows[4].astype(jnp.float32),
            read_conv_weight.astype(jnp.float32),
        )
    )
    discrete_step = jax.nn.softplus(step_raw + step_size_bias[None, :])
    step_logarithm = discrete_step * (-jnp.exp(log_decay_rate))[None, :] + decay_spikes.T
    heads_here = discrete_step.shape[1]
    groups_here = seq_write.shape[1] // STATE
    per_group = heads_here // groups_here
    blocks = length // PLAIN_BLOCK
    input_blocks = seq_input.reshape(blocks, PLAIN_BLOCK, heads_here, HEAD_DIM)
    weighted = input_blocks * discrete_step.reshape(blocks, PLAIN_BLOCK, heads_here, 1)
    write_blocks = jnp.repeat(
        seq_write.reshape(blocks, PLAIN_BLOCK, groups_here, STATE), per_group, axis=2
    )
    read_blocks = jnp.repeat(seq_read.reshape(blocks, PLAIN_BLOCK, groups_here, STATE), per_group, axis=2)
    cumulative = jnp.cumsum(step_logarithm.reshape(blocks, PLAIN_BLOCK, heads_here), axis=1)
    causal = lax.broadcasted_iota(jnp.int32, (PLAIN_BLOCK, PLAIN_BLOCK), 0) >= lax.broadcasted_iota(
        jnp.int32, (PLAIN_BLOCK, PLAIN_BLOCK), 1
    )
    scores = jnp.einsum("clhm,cshm->clsh", read_blocks, write_blocks, precision=highest)
    damping = jnp.exp(
        jnp.where(
            causal[None, :, :, None],
            cumulative[:, :, None, :] - cumulative[:, None, :, :],
            -jnp.inf,
        )
    )
    within_block = jnp.einsum("clsh,cshp->clhp", scores * damping, weighted, precision=highest)
    to_end = jnp.exp(cumulative[:, -1:, :] - cumulative)
    block_states = jnp.einsum(
        "cshm,cshp->chpm", write_blocks * to_end[..., None], weighted, precision=highest
    )
    block_logs = cumulative[:, -1, :]

    def advance(carried_state, inputs):
        contribution, block_log = inputs
        return (carried_state * jnp.exp(block_log)[:, None, None] + contribution, carried_state)

    own_total, own_before = lax.scan(
        advance, jnp.zeros(block_states.shape[1:], jnp.float32), (block_states, block_logs)
    )
    total_log = jnp.sum(block_logs, axis=0)
    arriving = prefix(
        (jnp.exp(total_log), own_total),
        "sp",
        combine_states,
        (jnp.ones_like(total_log), jnp.zeros_like(own_total)),
    )[1]
    before_logs = jnp.cumsum(block_logs, axis=0) - block_logs
    entering = own_before + jnp.exp(before_logs)[:, :, None, None] * arriving[None]
    from_before = (
        jnp.einsum("clhm,chpm->clhp", read_blocks, entering, precision=highest)
        * jnp.exp(cumulative)[..., None]
    )
    head_out = within_block + from_before + direct_path_weight[None, None, :, None] * input_blocks
    head_out = head_out.reshape(length, heads_here * HEAD_DIM)
    gated_heads = (head_out * jax.nn.silu(out_gate.astype(jnp.float32))).reshape(
        length, heads_here, HEAD_DIM
    )
    normalized = gated_heads * lax.rsqrt(
        jnp.mean(gated_heads * gated_heads, axis=2, keepdims=True) + epsilon
    )
    state_part = (
        normalized.reshape(length, heads_here * HEAD_DIM) * head_norm_scale.astype(jnp.float32)
    ).astype(jnp.bfloat16)
    wide_mixer, wide_state = (
        lax.all_gather(conv_output_weight, "sp", axis=1, tiled=True),
        lax.all_gather(state_output_weight, "sp", axis=1, tiled=True),
    )
    return lax.psum_scatter(
        (
            jnp.dot(mixer_part, wide_mixer, preferred_element_type=jnp.float32)
            + jnp.dot(state_part, wide_state, preferred_element_type=jnp.float32)
        ).astype(jnp.bfloat16),
        "tp",
        scatter_dimension=0,
        tiled=True,
    )


def per_device(
    tokens, input_norm_scale, outer_gate_weight, inner_gate_weight, value_weight_matrix,
    output_gate_weight, state_input_weight, write_key_weight, read_key_weight, step_size_weight,
    gated_conv_weight, input_conv_weight, write_conv_weight, read_conv_weight, step_size_bias,
    log_decay_rate, decay_spikes, direct_path_weight, head_norm_scale, conv_output_weight,
    state_output_weight,
):
    n, T = lax.axis_size("sp"), lax.axis_size("tp")
    rows, width = tokens.shape
    kdim, cdim = outer_gate_weight.shape
    heads = step_size_bias.shape[0]
    hw = heads * HEAD_DIM
    length = rows * T
    ocols = conv_output_weight.shape[1]
    if (
        kdim % 128 or ocols % 256 or n % 2 or n != 2 * PLANES or T % CORES
        or T < 2 * CORES
        or write_key_weight.shape[1] != STATE
    ):
        return plain_path(
            tokens, input_norm_scale, outer_gate_weight, inner_gate_weight,
            value_weight_matrix, output_gate_weight, state_input_weight, write_key_weight,
            read_key_weight, step_size_weight, gated_conv_weight, input_conv_weight,
            write_conv_weight, read_conv_weight, step_size_bias, log_decay_rate, decay_spikes,
            direct_path_weight, head_norm_scale, conv_output_weight, state_output_weight,
        )
    Y = T // CORES
    sm = pl.BlockSpec(memory_space=pltpu.SMEM)
    hbm = pl.BlockSpec(memory_space=pl.ANY)
    dma = pltpu.SemaphoreType.DMA
    s_cols, blocks = cdim + 2 * STATE, length // CHUNK

    def like(array):
        return pltpu.VMEM(array.shape, array.dtype)

    step_t = step_size_weight.T
    near, far = pl.pallas_call(
        functools.partial(kernel, n, T),
        out_shape=(
            jax.ShapeDtypeStruct((rows, width), bf16),
            jax.ShapeDtypeStruct((Y - 1, rows, width), bf16),
        ),
        in_specs=[hbm] * 14 + [sm] * 2 + [hbm, sm, hbm] + [hbm] * 2,
        out_specs=(hbm, hbm),
        scratch_shapes=[
            like(tokens),
            like(input_norm_scale),
            like(step_t),
            like(gated_conv_weight),
            like(input_conv_weight),
            like(write_conv_weight),
            like(read_conv_weight),
            like(decay_spikes),
            like(head_norm_scale),
            pltpu.VMEM((n, kdim, s_cols), bf16),
            pltpu.VMEM((n, kdim, cdim), bf16),
            pltpu.VMEM((n, kdim, 3 * cdim), bf16),
            pltpu.VMEM((n, cdim + hw, ocols), bf16),
            pltpu.VMEM((HALO + length, width), bf16),
            pltpu.VMEM((HALO + length, width), bf16),
            like(decay_spikes),
            pltpu.VMEM((2, HALO + length, s_cols), f32),
            pltpu.VMEM((2, HALO + length, cdim), f32),
            pltpu.VMEM((HALO + length, 3 * cdim), f32),
            pltpu.VMEM((2, length, hw), bf16),
            pltpu.VMEM((2, length, hw), f32),
            pltpu.VMEM((2, length, STATE), bf16),
            pltpu.VMEM((2, length, STATE), bf16),
            pltpu.VMEM((2, length, hw), f32),
            pltpu.VMEM((2, length, hw), f32),
            pltpu.VMEM((2, blocks, STATE, hw), f32),
            pltpu.VMEM((2, STATE, hw), f32),
            pltpu.VMEM((2, 1, hw), f32),
            pltpu.VMEM((2, STATE + HALO, hw), bf16),
            pltpu.VMEM((2, STATE + HALO, hw), bf16),
            pltpu.VMEM((STATE, hw), bf16),
            pltpu.VMEM((STATE, hw), bf16),
            pltpu.VMEM((length, hw), bf16),
            pltpu.VMEM((length, cdim + hw), bf16),
            pltpu.VMEM((n, length, ocols), bf16),
            pltpu.VMEM((n, Y, rows, ocols), bf16),
            pltpu.VMEM((Y - 1, n, rows, ocols), bf16),
            pltpu.VMEM((n, rows, ocols), bf16),
            dma((13,)),
            dma,
            dma(((n - 1) * PIECES_S,)),
            dma,
            dma(((n - 1) * PIECES_G,)),
            dma,
            dma(((n - 1) * PIECES_C,)),
            dma,
            dma,
            dma(((n - 1) * PIECES_O,)),
            dma,
            dma((Y, PIECES_T)),
            dma,
            dma((Y, PIECES_T)),
            dma,
            dma((PIECES_U,)),
            dma,
            dma((Y, PIECES_U)),
            dma,
            dma((Y, PIECES_U)),
            dma((2,)),
            dma((2,)),
            dma((2,)),
            dma((2,)),
            dma((2,)),
            dma((2,)),
            dma,
            dma((blocks,)),
            dma,
            dma((n,)),
            dma,
            dma,
            dma,
        ],
        compiler_params=pltpu.CompilerParams(
            collective_id=0, has_side_effects=True, vmem_limit_bytes=62 * 1024 * 1024
        ),
    )(
        tokens, input_norm_scale, outer_gate_weight, inner_gate_weight,
        value_weight_matrix, output_gate_weight, state_input_weight, write_key_weight,
        read_key_weight, step_t, gated_conv_weight, input_conv_weight, write_conv_weight,
        read_conv_weight, step_size_bias, log_decay_rate, decay_spikes, direct_path_weight,
        head_norm_scale,
        conv_output_weight, state_output_weight,
    )
    total = near.astype(f32)
    for d in range(Y - 1):
        total = total + far[d].astype(f32)
    return total.astype(bf16)


def solution(mesh):
    placed = (
        (P(("sp", "tp"), None), P())
        + (P("sp", "tp"),) * 7
        + (P(None, "tp"),) * 5
        + (P("tp"), P("tp"), P("tp", "sp"), P("tp"), P("tp"), P("tp", "sp"), P("tp", "sp"))
    )
    return jax.shard_map(
        per_device, mesh=mesh, in_specs=placed, out_specs=P(("sp", "tp"), None), check_vma=False
    )
```

time: 97.7 us -> 88.3 us (0.904)
  Pallas kernels: 95.4 us -> 86 us
    pallas_call x1, Pallas kernels: 95.4 us -> 86 us  [per_device(): pl.pallas_call(functools.partial(kernel, n, T), out_shape=(jax.ShapeDtype...]
where the time goes in v3:
time: 88.3 us; the launch traced here: 88.1 us
  Pallas kernels  86 us (97%)
  other arithmetic  2.12 us (2%)
    pallas_call x1, Pallas kernels, per_device(): pl.pallas_call(functools.partial(kernel, n, T), out_shape=(jax.ShapeDtype...  86 us
    convert_element_type x1, other arithmetic, per_device(): return total.astype(bf16)  2.12 us

profile of v3, /device:TPU:0, one launch (start us, length us, event | category | flops | bytes accessed | tf_op | source)
XLA Modules:
  0.0 88.1 jit_solution(8846018060589411370)
XLA Ops:
  0.0 86.0 %shard_map.199 = (bf16[128,2048]{1,0:T(8,128)(2,1)}, bf16[1,128,2048]{2,1,0:T(8,128)(2,1)}) custom-call(bf16[128,2048]{1,0:T(8,128)(2,1)} %tokens_h.1, bf16[2048]{0:T(1024)(128)(2,1)} %in_scale_h.1, bf16[256,256]{1,0:T(8,128)(2,1)} %w_outer.1, bf16[256,256]{1,0:T(8,128)(2,1)} %w_inner.1, bf16[256,256]{1,0:T(8,128)(2,1)} %w_value.1, ...), custom_call_target="tpu_custom_call" | custom-call | tf_op jit(solution)/shard_map/pallas_call | solution.py:1105
  86.0 2.1 %fusion = bf16[128,2048]{1,0:T(8,128)(2,1)} fusion(bf16[128,2048]{1,0:T(8,128)(2,1)} %get-tuple-element.7, bf16[1,128,2048]{2,1,0:T(8,128)(2,1)} %get-tuple-element.8), kind=kLoop, calls=%fused_computation.1 | loop fusion | flops 1048576 | bytes 1572864 | tf_op jit(solution)/shard_map/convert_element_type | solution.py:1200

commit v4 on v3

--- a/solution.py
+++ b/solution.py
@@ -12,8 +12,8 @@
 PLAIN_BLOCK = 64
 CHUNK = 128
 HALO = 16
-PIECES_S = 4
-PIECES_G = 2
+PIECES_S = 2
+PIECES_G = 1
 PIECES_C = 4
 PIECES_O = 2
 PIECES_T = 2
@@ -73,10 +73,10 @@
     T,
     tokens_h, in_scale_h, w_outer, w_inner, w_value, w_ogate, w_state, w_write, w_read,
     step_w_h, taps_conv_h, taps_in_h, taps_wr_h, taps_rd_h,
-    bias, rate, spikes_h, direct, hscale_h, o_conv, o_state,
+    bias_h, rate_h, spikes_h, direct_h, hscale_h, o_conv, o_state,
     near, far,
     tokens, in_scale, step_w, taps_conv, taps_in, taps_wr, taps_rd, spikes, hscale,
-    sbuf, gbuf, cbuf, obuf, norm, norm2, spikes2, acc_s, acc_g, acc_c,
+    bias, rate, direct, sbuf, gbuf, cbuf, obuf, norm, norm2, spikes2, acc_s, acc_g, acc_c,
     mixbuf, xbuf, wrbuf, rdbuf, ybuf, cumbuf, stbuf, runbuf, decbuf,
     st_send, st_recv, e_send, e_recv, mbuf, apart, part, r1, p2, nbuf,
     loc_sem, ss_sem, sr_sem, gs_sem, gr_sem, cs_sem, cr_sem, os_sem, ox_sem, or_sem,
@@ -124,6 +124,7 @@
         "v": [
             (spikes_h, spikes), (step_w_h, step_w), (taps_conv_h, taps_conv),
             (taps_in_h, taps_in), (taps_wr_h, taps_wr), (taps_rd_h, taps_rd), (hscale_h, hscale),
+            (bias_h, bias), (rate_h, rate), (direct_h, direct),
         ],
         "o": pack((o_conv, o_state), obuf, True),
     }
@@ -199,14 +200,11 @@
         def piece(self, slot, q):
             return cbuf.at[slot, pl.ds(q * self.rows, self.rows)]
 
-        def has(self, link, s, q):
-            return s < n // 2 - 1 or (q < PIECES_C // 2) == (link == 0)
-
         def copy(self, link, s, q):
             src = 0 if s == 0 else ring_slot(1 - link, s)
             dst = ring_slot(link, s + 1)
             return remote(
-                self.piece(src, q), self.piece(dst, q), cs_sem,
+                self.piece(src, q), self.piece(dst, q), cs_sem.at[s // (n // 2 - 1)],
                 cr_sem.at[(dst - 1) * PIECES_C + q], {"sp": link_device[link]},
             )
 
@@ -214,7 +212,7 @@
             if (slot, q) not in self.waited:
                 self.waited.add((slot, q))
                 remote(
-                    self.piece(slot, q), self.piece(slot, q), cs_sem,
+                    self.piece(slot, q), self.piece(slot, q), cs_sem.at[0],
                     cr_sem.at[(slot - 1) * PIECES_C + q], {"sp": mate},
                 ).wait_recv()
 
@@ -282,7 +280,7 @@
         return remote(src, u_rows(tp, q), vs_sem, vr_sem.at[q], {"sp": mate})
 
     def k_copy():
-        cut = pl.ds(0, HALO)
+        cut = pl.ds(HALO - 8, 8)
         return remote(norm.at[cut], norm2.at[cut], k_sem.at[0], k_sem.at[1], {"sp": mate})
 
     def l_copy():
@@ -371,15 +369,24 @@
             ring.need(slot)
         project(acc_c, norm, cbuf, slots, ring_owner, s == 0)
 
-    def conv_mix():
-        for b in range(blocks):
-            span, own, take = spans(b)
+    half_rows = length // Y
+    half_blocks = half_rows // CHUNK
+
+    def conv_mix(y):
+        for b in range(half_blocks):
+            t0 = y * half_rows + b * CHUNK
+            span = pl.ds(pl.multiple_of(t0, CHUNK), CHUNK)
+            own = pl.ds(pl.multiple_of(t0 + HALO, HALO), CHUNK)
+            take = pl.ds(pl.multiple_of(t0 + HALO - 8, 8), CHUNK + 8)
             product = field(acc_c, cdim, cdim, take) * field(acc_c, 2 * cdim, cdim, take)
             mix = field(acc_c, 0, cdim, own) * taps(product, taps_conv)
             apart[span, 0:cdim] = mix.astype(bf16)
 
+    def turned(b):
+        return lax.rem(b + (1 - chip) * half_blocks, blocks)
+
     def m_copy(b):
-        cut = pl.ds(b * CHUNK, CHUNK)
+        cut = pl.ds(pl.multiple_of(turned(b) * CHUNK, CHUNK), CHUNK)
         return remote(
             mbuf.at[cut], apart.at[cut, pl.ds(cdim, heads_width)], ms_sem, mr_sem.at[b],
             {"sp": mate},
@@ -400,7 +407,7 @@
         step_two = sorted((q + 2.5 * link, link, q) for link in (0, 1) for q in range(PIECES_C))
         forwards += [(link, 2, q) for _, link, q in step_two]
         for q in range(PIECES_C // 2):
-            forwards += [(0, 3, q), (1, 3, PIECES_C // 2 + q)]
+            forwards += [(1, 3, PIECES_C // 2 + q)]
         done = [0]
 
         def pump(count):
@@ -549,6 +556,10 @@
                 ol.send(slot, 4 + slot, q, ox_sem, side)
         for b in range(blocks):
             within(0, b)
+        for q in range(PIECES_O):
+            ol.arrive(1, q, os_sem, mate)
+            ol.send(1, 3, q, os_sem, cross)
+            ol.send(1, 5, q, ox_sem, side)
         pump(1)
         x_copy().wait_recv()
         second = jnp.broadcast_to(x, (1, heads_width)) == 1
@@ -580,10 +591,6 @@
             decbuf[1] = first_decay[1] * pair_decay[0]
 
         pump(2)
-        for q in range(PIECES_O):
-            ol.arrive(1, q, os_sem, mate)
-            ol.send(1, 3, q, os_sem, cross)
-            ol.send(1, 5, q, ox_sem, side)
         pump(1)
         for slot in range(1, n - 1):
             for q in range(PIECES_G):
@@ -598,6 +605,11 @@
         for k, source in enumerate((norm, norm2)):
             project(acc_g.at[k], source, gbuf, (n - 1,), plane_owner)
 
+        for q in range(PIECES_O):
+            ol.arrive(3, q, os_sem, mate)
+            ol.send(3, 3, q, os_sem, mate)
+            ol.send(3, 7, q, ox_sem, side)
+
         @pl.when(upper == 1)
         def _():
             e_copy().wait_recv()
@@ -616,14 +628,19 @@
         for k in (1, 0):
             so_far = jnp.zeros((1, heads_width), f32)
             for b in range(blocks):
-                span, own, _ = spans(b)
-                cum_wide = cumbuf[k, span, :]
-                entering = (stbuf[k, b] + jnp.exp(so_far) * runbuf[k]).astype(bf16)
-                so_far = so_far + cum_wide[CHUNK - 1 : CHUNK]
+                stbuf[k, b] = stbuf[k, b] + jnp.exp(so_far) * runbuf[k]
+                at_end = b * CHUNK + CHUNK - 1
+                so_far = so_far + cumbuf[k, at_end : at_end + 1, :]
+            for i in range(blocks):
+                b = turned(i)
+                span = pl.ds(pl.multiple_of(b * CHUNK, CHUNK), CHUNK)
+                own = pl.ds(pl.multiple_of(b * CHUNK + HALO, HALO), CHUNK)
                 head_out = (
                     ybuf[k, span, :]
-                    + jnp.dot(rdbuf[k, span, :], entering, preferred_element_type=f32)
-                    * jnp.exp(cum_wide)
+                    + jnp.dot(
+                        rdbuf[k, span, :], stbuf[k, b].astype(bf16), preferred_element_type=f32
+                    )
+                    * jnp.exp(cumbuf[k, span, :])
                     + direct_wide * xbuf[k, span, :]
                 )
                 gated = head_out * silu(field(acc_g.at[k], 0, cdim, own))
@@ -634,7 +651,7 @@
                 ).astype(bf16)
                 if k == 1:
                     mbuf[span, :] = result
-                    m_copy(b).start()
+                    m_copy(i).start()
                 else:
                     apart[span, cdim:] = result
         pump(1)
@@ -642,13 +659,9 @@
         pump(1)
         conv_step(ring, 2)
         pump(len(forwards))
-        for q in range(PIECES_O):
-            ol.arrive(3, q, os_sem, mate)
-            ol.send(3, 3, q, os_sem, mate)
-            ol.send(3, 7, q, ox_sem, side)
         conv_step(ring, 3)
         conv_step(ring, n // 2)
-        conv_mix()
+        conv_mix(1 - chip)
 
     def blocks_sent(buf, count, sem):
         every = buf.at[pl.ds(0, count)]
@@ -700,15 +713,15 @@
         for q in range(PIECES_O):
             ol.arrive(2, q, os_sem, mate)
             ol.send(2, 6, q, ox_sem, side)
-        for q in range(PIECES_C // 2, PIECES_C):
+        for q in range(PIECES_C):
             ring.forward(1, 3, q)
         conv_step(ring, 3)
+        conv_step(ring, n // 2)
+        conv_mix(1 - chip)
         for q in range(PIECES_O):
             ol.arrive(3, q, os_sem, mate)
             ol.send(3, 7, q, ox_sem, side)
-        conv_step(ring, n // 2)
-        conv_mix()
-        for b in range(blocks):
+        for b in range(half_blocks):
             m_copy(b).wait_recv()
 
     landed("s")
@@ -720,6 +733,10 @@
         for q in range(PIECES_S):
             first_s.send(0, 2, q, ss_sem, cross)
             first_s.send(0, 4, q, ss_sem, side)
+
+    @pl.when(is_inner)
+    def _():
+        norm2[0 : HALO - 8, :] = jnp.zeros((HALO - 8, width), bf16)
 
     @pl.when(z == end_z)
     def _():
@@ -758,7 +775,7 @@
     def r1_copy(d, s):
         return remote(
             part.at[s, block_rows(lax.rem(chip + d, Y), 1 - core)], r1.at[s, d], r1s_sem,
-            r1r_sem.at[s], {"tp": partner},
+            r1r_sem.at[d, s], {"tp": partner},
         )
 
     def r2_copy(d, s):
@@ -772,35 +789,50 @@
 
     o_last = Slots(obuf, PIECES_O, or_sem)
 
-    def project_out(s):
+    def project_out(d, s):
         if s >= 4:
             for q in range(PIECES_O):
                 o_last.arrive(s, q, os_sem, mate)
-        part[s] = jnp.dot(apart[...], obuf[s], preferred_element_type=f32).astype(bf16)
-        for d in range(1, Y):
-            r1_copy(d, s).start()
-        r1_copy(0, s).start()
-
-    def reduce(s):
-        remote(r1.at[s], r1.at[s], r1s_sem, r1r_sem.at[s], {"tp": partner}).wait_recv()
-        for d in range(1, Y):
-            mine = part[s, block_rows(lax.rem(chip + d, Y), core), :]
-            p2[d - 1, s] = (mine.astype(f32) + r1[s, d].astype(f32)).astype(bf16)
+        span = pl.ds(pl.multiple_of(lax.rem(chip + d, Y) * half_rows, half_rows), half_rows)
+        part[s, span, :] = jnp.dot(
+            apart[span, :], obuf[s], preferred_element_type=f32
+        ).astype(bf16)
+        r1_copy(d, s).start()
+
+    def reduce(d, s):
+        r1_copy(d, s).wait_recv()
+        mine = part[s, block_rows(lax.rem(chip + d, Y), core), :]
+        total = (mine.astype(f32) + r1[s, d].astype(f32)).astype(bf16)
+        if d:
+            p2[d - 1, s] = total
             r2_copy(d, s).start()
-        mine = part[s, block_rows(chip, core), :]
-        nbuf[s] = (mine.astype(f32) + r1[s, 0].astype(f32)).astype(bf16)
-        near_copy(s).start()
-
-    order = [0, 1, 2, 4, 5, 6, 3, 7]
-    previous = None
-    for slot in order:
-        if slot == order[-1]:
-            reduce(previous)
-        project_out(slot)
-        if slot != order[-1] and previous is not None:
-            reduce(previous)
-        previous = slot
-    reduce(previous)
+        else:
+            nbuf[s] = total
+            near_copy(s).start()
+
+    open_sums = []
+
+    def output(d, s, lag=3):
+        project_out(d, s)
+        open_sums.append((d, s))
+        if len(open_sums) > lag:
+            reduce(*open_sums.pop(0))
+
+    for s in (0, 1, 2, 4, 5, 6):
+        output(1, s)
+    conv_mix(chip)
+
+    @pl.when(z == end_z)
+    def _():
+        for b in range(half_blocks, blocks):
+            m_copy(b).wait_recv()
+
+    while open_sums:
+        reduce(*open_sums.pop(0))
+    for d, s in ((0, 0), (0, 1), (1, 3), (0, 2), (0, 4), (1, 7), (0, 5), (0, 6), (0, 3), (0, 7)):
+        output(d, s, 1 if s == 7 else 2)
+    while open_sums:
+        reduce(*open_sums.pop(0))
 
     @pl.when(is_inner)
     def _():
@@ -810,6 +842,8 @@
         def _():
             e_copy().wait_send()
 
+        half = cbuf.at[pl.ds(0, 1), pl.ds(0, kdim // 2)]
+        remote(half, half, cs_sem.at[1], cr_sem.at[0], {"sp": mate}).wait_send()
         blocks_sent(sbuf, 6, ss_sem)
         blocks_sent(gbuf, 6, gs_sem)
         blocks_sent(obuf, 5, os_sem)
@@ -825,6 +859,8 @@
 
     @pl.when(z == end_z)
     def _():
+        half = cbuf.at[pl.ds(0, 3), pl.ds(0, kdim // 2)]
+        remote(half, half, cs_sem.at[1], cr_sem.at[0], {"sp": mate}).wait_send()
         blocks_sent(sbuf, 1, ss_sem)
         blocks_sent(gbuf, 1, gs_sem)
         blocks_sent(obuf, 1, os_sem)
@@ -834,7 +870,7 @@
         k_copy().wait_send()
         l_copy().wait_send()
 
-    blocks_sent(cbuf, n - 1, cs_sem)
+    blocks_sent(cbuf, n - 2, cs_sem.at[0])
     blocks_sent(obuf, 4, ox_sem)
     remote(
         norm.at[pl.ds(0, Y * rows)], norm.at[pl.ds(0, Y * rows)], ts_sem, tr_sem.at[0, 0],
@@ -854,7 +890,7 @@
         cut = pl.ds(0, (T - 1) * HALO)
         remote(norm.at[cut], norm.at[cut], g_sem.at[0], g_sem.at[1], {"tp": partner}).wait_send()
 
-    remote(r1, r1, r1s_sem, r1r_sem.at[0], {"tp": partner}).wait_send()
+    remote(r1, r1, r1s_sem, r1r_sem.at[0, 0], {"tp": partner}).wait_send()
     remote(p2, p2, r2s_sem, r2r_sem, {"tp": partner}).wait_send()
     pltpu.make_async_copy(far.at[0], near, near_sem).wait()
     remote(far, far, r2s_sem, r2r_sem, {"tp": partner}).wait_recv()
@@ -1082,7 +1118,7 @@
     ocols = conv_output_weight.shape[1]
     if (
         kdim % 128 or ocols % 256 or n % 2 or n != 2 * PLANES or T % CORES
-        or T < 2 * CORES
+        or T != 2 * CORES
         or write_key_weight.shape[1] != STATE
     ):
         return plain_path(
@@ -1093,7 +1129,6 @@
             direct_path_weight, head_norm_scale, conv_output_weight, state_output_weight,
         )
     Y = T // CORES
-    sm = pl.BlockSpec(memory_space=pltpu.SMEM)
     hbm = pl.BlockSpec(memory_space=pl.ANY)
     dma = pltpu.SemaphoreType.DMA
     s_cols, blocks = cdim + 2 * STATE, length // CHUNK
@@ -1108,7 +1143,7 @@
             jax.ShapeDtypeStruct((rows, width), bf16),
             jax.ShapeDtypeStruct((Y - 1, rows, width), bf16),
         ),
-        in_specs=[hbm] * 14 + [sm] * 2 + [hbm, sm, hbm] + [hbm] * 2,
+        in_specs=[hbm] * 21,
         out_specs=(hbm, hbm),
         scratch_shapes=[
             like(tokens),
@@ -1120,6 +1155,9 @@
             like(read_conv_weight),
             like(decay_spikes),
             like(head_norm_scale),
+            pltpu.SMEM((heads,), f32),
+            pltpu.SMEM((heads,), f32),
+            pltpu.SMEM((heads,), f32),
             pltpu.VMEM((n, kdim, s_cols), bf16),
             pltpu.VMEM((n, kdim, cdim), bf16),
             pltpu.VMEM((n, kdim, 3 * cdim), bf16),
@@ -1149,12 +1187,12 @@
             pltpu.VMEM((n, Y, rows, ocols), bf16),
             pltpu.VMEM((Y - 1, n, rows, ocols), bf16),
             pltpu.VMEM((n, rows, ocols), bf16),
-            dma((13,)),
+            dma((16,)),
             dma,
             dma(((n - 1) * PIECES_S,)),
             dma,
             dma(((n - 1) * PIECES_G,)),
-            dma,
+            dma((2,)),
             dma(((n - 1) * PIECES_C,)),
             dma,
             dma,
@@ -1178,7 +1216,7 @@
             dma,
             dma((blocks,)),
             dma,
-            dma((n,)),
+            dma((Y, n)),
             dma,
             dma,
             dma,

time: 88.3 us -> 83.1 us (0.941)
  the two profiles are of different devices: /device:TPU:0 before, /device:TPU:16 now
where the time goes in v4:
time: 83.1 us; the launch traced here: 83 us
  Pallas kernels  80.8 us (97%)
  other arithmetic  2.12 us (3%)
    pallas_call x1, Pallas kernels, per_device(): pl.pallas_call(functools.partial(kernel, n, T), out_shape=(jax.ShapeDtype...  80.8 us
    convert_element_type x1, other arithmetic, per_device(): return total.astype(bf16)  2.12 us

profile of v4, /device:TPU:16, one launch (start us, length us, event | category | flops | bytes accessed | tf_op | source)
XLA Modules:
  0.0 83.0 jit_solution(17881020194242190365)
XLA Ops:
  0.0 80.8 %shard_map.199 = (bf16[128,2048]{1,0:T(8,128)(2,1)}, bf16[1,128,2048]{2,1,0:T(8,128)(2,1)}) custom-call(bf16[128,2048]{1,0:T(8,128)(2,1)} %tokens_h.1, bf16[2048]{0:T(1024)(128)(2,1)} %in_scale_h.1, bf16[256,256]{1,0:T(8,128)(2,1)} %w_outer.1, bf16[256,256]{1,0:T(8,128)(2,1)} %w_inner.1, bf16[256,256]{1,0:T(8,128)(2,1)} %w_value.1, ...), custom_call_target="tpu_custom_call" | custom-call | tf_op jit(solution)/shard_map/pallas_call | solution.py:1140
  80.8 2.1 %fusion = bf16[128,2048]{1,0:T(8,128)(2,1)} fusion(bf16[128,2048]{1,0:T(8,128)(2,1)} %get-tuple-element.7, bf16[1,128,2048]{2,1,0:T(8,128)(2,1)} %get-tuple-element.8), kind=kLoop, calls=%fused_computation.1 | loop fusion | flops 1048576 | bytes 1572864 | tf_op jit(solution)/shard_map/convert_element_type | solution.py:1238

commit v5 on v4

--- a/solution.py
+++ b/solution.py
@@ -19,6 +19,7 @@
 PIECES_T = 2
 PIECES_U = 4
 PLANES = 4
+FAR_PIECES = 1
 CORES = 2
 epsilon = 1e-05
 highest = lax.Precision.HIGHEST
@@ -407,7 +408,8 @@
         step_two = sorted((q + 2.5 * link, link, q) for link in (0, 1) for q in range(PIECES_C))
         forwards += [(link, 2, q) for _, link, q in step_two]
         for q in range(PIECES_C // 2):
-            forwards += [(1, 3, PIECES_C // 2 + q)]
+            if q < FAR_PIECES:
+                forwards += [(1, 3, PIECES_C - FAR_PIECES + q)]
         done = [0]
 
         def pump(count):
@@ -605,11 +607,6 @@
         for k, source in enumerate((norm, norm2)):
             project(acc_g.at[k], source, gbuf, (n - 1,), plane_owner)
 
-        for q in range(PIECES_O):
-            ol.arrive(3, q, os_sem, mate)
-            ol.send(3, 3, q, os_sem, mate)
-            ol.send(3, 7, q, ox_sem, side)
-
         @pl.when(upper == 1)
         def _():
             e_copy().wait_recv()
@@ -652,6 +649,11 @@
                 if k == 1:
                     mbuf[span, :] = result
                     m_copy(i).start()
+                    if i == half_blocks - 1:
+                        for q in range(PIECES_O):
+                            ol.arrive(3, q, os_sem, mate)
+                            ol.send(3, 3, q, os_sem, mate)
+                            ol.send(3, 7, q, ox_sem, side)
                 else:
                     apart[span, cdim:] = result
         pump(1)
@@ -707,7 +709,7 @@
         conv_step(ring, 1)
         for q in range(PIECES_C):
             ring.forward(1, 2, q)
-        for q in range(PIECES_C // 2):
+        for q in range(PIECES_C - FAR_PIECES):
             ring.forward(0, 3, q)
         conv_step(ring, 2)
         for q in range(PIECES_O):
@@ -718,9 +720,6 @@
         conv_step(ring, 3)
         conv_step(ring, n // 2)
         conv_mix(1 - chip)
-        for q in range(PIECES_O):
-            ol.arrive(3, q, os_sem, mate)
-            ol.send(3, 7, q, ox_sem, side)
         for b in range(half_blocks):
             m_copy(b).wait_recv()
 
@@ -818,12 +817,16 @@
         if len(open_sums) > lag:
             reduce(*open_sums.pop(0))
 
-    for s in (0, 1, 2, 4, 5, 6):
-        output(1, s)
+    for s in (0, 1, 2, 4, 6, 5):
+        output(1, s, 1)
     conv_mix(chip)
 
     @pl.when(z == end_z)
     def _():
+        ol = Slots(obuf, PIECES_O, or_sem)
+        for q in range(PIECES_O):
+            ol.arrive(3, q, os_sem, mate)
+            ol.send(3, 7, q, ox_sem, side)
         for b in range(half_blocks, blocks):
             m_copy(b).wait_recv()
 
@@ -842,8 +845,8 @@
         def _():
             e_copy().wait_send()
 
-        half = cbuf.at[pl.ds(0, 1), pl.ds(0, kdim // 2)]
-        remote(half, half, cs_sem.at[1], cr_sem.at[0], {"sp": mate}).wait_send()
+        last_hop = cbuf.at[pl.ds(0, FAR_PIECES), pl.ds(0, kdim // PIECES_C)]
+        remote(last_hop, last_hop, cs_sem.at[1], cr_sem.at[0], {"sp": mate}).wait_send()
         blocks_sent(sbuf, 6, ss_sem)
         blocks_sent(gbuf, 6, gs_sem)
         blocks_sent(obuf, 5, os_sem)
@@ -859,8 +862,8 @@
 
     @pl.when(z == end_z)
     def _():
-        half = cbuf.at[pl.ds(0, 3), pl.ds(0, kdim // 2)]
-        remote(half, half, cs_sem.at[1], cr_sem.at[0], {"sp": mate}).wait_send()
+        last_hop = cbuf.at[pl.ds(0, 2 * PIECES_C - FAR_PIECES), pl.ds(0, kdim // PIECES_C)]
+        remote(last_hop, last_hop, cs_sem.at[1], cr_sem.at[0], {"sp": mate}).wait_send()
         blocks_sent(sbuf, 1, ss_sem)
         blocks_sent(gbuf, 1, gs_sem)
         blocks_sent(obuf, 1, os_sem)

time: 83.1 us -> 82.7 us (level)
  the two profiles are of different devices: /device:TPU:16 before, /device:TPU:11 now
where the time goes in v5:
time: 82.7 us; the launch traced here: 82.5 us
  Pallas kernels  80.4 us (97%)
  other arithmetic  2.12 us (3%)
    pallas_call x1, Pallas kernels, per_device(): pl.pallas_call(functools.partial(kernel, n, T), out_shape=(jax.ShapeDtype...  80.4 us
    convert_element_type x1, other arithmetic, per_device(): return total.astype(bf16)  2.12 us

profile of v5, /device:TPU:11, one launch (start us, length us, event | category | flops | bytes accessed | tf_op | source)
XLA Modules:
  0.0 82.5 jit_solution(7619679062156421894)
XLA Ops:
  0.0 80.4 %shard_map.199 = (bf16[128,2048]{1,0:T(8,128)(2,1)}, bf16[1,128,2048]{2,1,0:T(8,128)(2,1)}) custom-call(bf16[128,2048]{1,0:T(8,128)(2,1)} %tokens_h.1, bf16[2048]{0:T(1024)(128)(2,1)} %in_scale_h.1, bf16[256,256]{1,0:T(8,128)(2,1)} %w_outer.1, bf16[256,256]{1,0:T(8,128)(2,1)} %w_inner.1, bf16[256,256]{1,0:T(8,128)(2,1)} %w_value.1, ...), custom_call_target="tpu_custom_call" | custom-call | tf_op jit(solution)/shard_map/pallas_call | solution.py:1143
  80.4 2.1 %fusion = bf16[128,2048]{1,0:T(8,128)(2,1)} fusion(bf16[128,2048]{1,0:T(8,128)(2,1)} %get-tuple-element.7, bf16[1,128,2048]{2,1,0:T(8,128)(2,1)} %get-tuple-element.8), kind=kLoop, calls=%fused_computation.1 | loop fusion | flops 1048576 | bytes 1572864 | tf_op jit(solution)/shard_map/convert_element_type | solution.py:1241
